TPU v7x, 512 devices: a whole 4x4x16 slice. The times are simulated.
512 devices in a mesh: sp: 64 (over z, y), tp: 8 (over x, core).
Axes of the slice: x: 4, y: 4, z: 16, core: 2. Of those that a mesh axis runs over, the one named last changes fastest.
Arguments:
- receptance: bfloat16 [12288, 1024], P('sp', 'tp'), may hold values from -6 to 6
- head_keys: bfloat16 [12288, 1024], P('sp', 'tp'), may hold values from -6 to 6
- head_values: bfloat16 [12288, 1024], P('sp', 'tp'), may hold values from -6 to 6
- decay_preact: float32 [12288, 1024], P('sp', 'tp'), may hold values from -13.5 to -0.5
- learning_rate_preact: float32 [12288, 1024], P('sp', 'tp'), may hold values from -10.5 to 2.5
- output_gate_preact: bfloat16 [12288, 1024], P('sp', 'tp'), may hold values from -8 to 8
- self_token_weight: float32 [16, 64], P('tp'), may hold values from -0.6 to 0.6
- head_norm_gain: float32 [1024], P('tp'), may hold values from 0.1 to 1.9
- output_weight: bfloat16 [1024, 2048], P('tp'), may hold values from -0.1875 to 0.1875
- residual: bfloat16 [12288, 2048], P('sp'), may hold values from -6 to 6
- premixer_norm_gain: float32 [2048], replicated, may hold values from 0.1 to 1.9
- mixer_gate_weight: bfloat16 [2048, 5120], P('sp', 'tp'), may hold values from -0.125 to 0.125
- mixer_up_weight: bfloat16 [2048, 5120], P('sp', 'tp'), may hold values from -0.125 to 0.125
- mixer_down_weight: bfloat16 [5120, 2048], P('tp', 'sp'), may hold values from -0.078125 to 0.078125
Outputs:
- layer_out: bfloat16 [12288, 2048], P(('sp', 'tp'))
All inputs are finite; a program needn't handle non-finite values.
Results may differ from a plain program's by a relative error of at most 0.015.
Values may be sent and summed in bfloat16 or wider, within the bound.
A program may use at most 64 MiB of HBM per device.

v0:
```python
import jax
import jax.numpy as jnp
from jax import lax
from jax.sharding import Mesh
from jax.sharding import PartitionSpec as P

HEAD_SIZE = 64
SUB = 16
SP = ("sp_0", "sp_1")
SP_TP = ("sp_0", "sp_1", "tp")


GROUP_EPS = 0.00064
NORM_EPS = 1e-06
EXACT = lax.Precision.HIGHEST


def neutral_like(x, identity):
    return jax.tree.map(
        lambda part, zero: jnp.zeros_like(part) + jnp.asarray(zero, part.dtype), x, identity
    )


def gathered_once(x, axis):
    leaves = jax.tree.leaves(x)
    turns = sorted(range(len(leaves)), key=lambda k: -leaves[k].size)
    width = (1, *leaves[turns[0]].shape)[-1]
    lines = [
        jnp.pad(leaves[k].reshape(-1), (0, -leaves[k].size % width)).reshape(-1, width)
        for k in turns
    ]
    both, at, found = (lax.all_gather(jnp.concatenate(lines), axis), 0, {})
    for k, line in zip(turns, lines):
        piece = both[:, at : at + len(line)].reshape(len(both), -1)
        found[k] = piece[:, : leaves[k].size].reshape(-1, *leaves[k].shape)
        at += len(line)
    numbers = iter(range(len(leaves)))
    return jax.tree.map(lambda _: found[next(numbers)], x)


def entering(x, axes, combine, identity):
    before = start = neutral_like(x, identity)
    running = x
    for axis in reversed(axes):
        length, here = (lax.axis_size(axis), lax.axis_index(axis))
        pieces = gathered_once(running, axis)
        inside, running = (start, start)
        for k in range(length):
            passed = k < here
            running = combine(running, jax.tree.map(lambda part: part[k], pieces))
            inside = jax.tree.map(lambda new, old: jnp.where(passed, new, old), running, inside)
        before = combine(inside, before)
    return before


def split_up(x, dim, length):
    shape = x.shape
    tiles = x.reshape(*shape[:dim], length, shape[dim] // length, *shape[dim + 1 :])
    return jnp.moveaxis(tiles, dim, 0)


def summed_on_arrival(x, axis, dim):
    length = lax.axis_size(axis)
    tiles = lax.all_to_all(split_up(x, dim, length), axis, 0, 0, tiled=True)
    return jnp.sum(tiles.astype(jnp.float32), axis=0)


def joined_along(tiles, dim):
    shape = list(tiles.shape[1:])
    shape[dim] *= tiles.shape[0]
    return jnp.moveaxis(tiles, 0, dim).reshape(shape)


def from_everyone(x, axis):
    copies = jnp.broadcast_to(x, (lax.axis_size(axis), *x.shape))
    return lax.all_to_all(copies, axis, split_axis=0, concat_axis=0, tiled=True)


def gather_directly(x, axis, dim):
    return joined_along(from_everyone(x, axis), dim)


def sent_together(arrays, axis, dim, along):
    both = jnp.concatenate(arrays, axis=along)
    out, at, done = (lax.all_gather(both, axis, axis=dim, tiled=True), 0, [])
    for a in arrays:
        done.append(lax.slice_in_dim(out, at, at + a.shape[along], axis=along))
        at += a.shape[along]
    return tuple(done)


def gather_axes(x, axes, dim):
    for axis in reversed(axes):
        x = lax.all_gather(x, axis, axis=dim, tiled=True)
    return x


def compose(earlier, latter):
    product = jnp.einsum("...ij,...jk->...ik", earlier[0], latter[0], precision=EXACT)
    carried = jnp.einsum("...ij,...jk->...ik", earlier[1], latter[0], precision=EXACT) + latter[1]
    return (product, carried)


def final_output(
    layer_result,
    receptance_rows,
    keys_single,
    values_single,
    self_token_weight,
    head_norm_gain,
    output_gate_preact,
):
    centre = jnp.mean(layer_result, axis=-1, keepdims=True)
    spread = jnp.mean(jnp.square(layer_result - centre), axis=-1, keepdims=True)
    scaled_rows = (layer_result - centre) * lax.rsqrt(spread + GROUP_EPS)
    self_token_term = (
        jnp.sum(receptance_rows * keys_single * self_token_weight[None], axis=-1, keepdims=True)
        * values_single
    )
    sequence_length = layer_result.shape[0]
    heads_merged = scaled_rows.reshape(sequence_length, -1) * head_norm_gain[
        None
    ] + self_token_term.reshape(sequence_length, -1)
    return (heads_merged * jax.nn.sigmoid(output_gate_preact.astype(jnp.float32))).astype(
        jnp.bfloat16
    )


def rms_scale(row_block, gain_vec):
    widened = row_block.astype(jnp.float32)
    factor = lax.rsqrt(jnp.mean(widened * widened, axis=-1, keepdims=True) + NORM_EPS)
    return (widened * factor * gain_vec[None]).astype(jnp.bfloat16)


def per_device(
    receptance,
    head_keys,
    head_values,
    decay_preact,
    learning_rate_preact,
    output_gate_preact,
    self_token_weight,
    head_norm_gain,
    output_weight,
    residual,
    premixer_norm_gain,
    mixer_gate_weight,
    mixer_up_weight,
    mixer_down_weight,
):
    sequence_length = receptance.shape[0]
    head_count = receptance.shape[1] // HEAD_SIZE
    blocks = sequence_length // SUB
    layout = (sequence_length, head_count, HEAD_SIZE)
    receptance_rows = receptance.astype(jnp.float32).reshape(layout)
    keys_single = head_keys.astype(jnp.float32).reshape(layout)
    values_single = head_values.astype(jnp.float32).reshape(layout)
    decay_rate = jnp.exp(-jnp.exp(-jax.nn.softplus(-decay_preact) - 0.5)).reshape(layout)
    learn_rate = jax.nn.sigmoid(learning_rate_preact).reshape(layout)
    unit_key = keys_single / jnp.maximum(jnp.linalg.norm(keys_single, axis=-1, keepdims=True), 1.0)
    remove_dir = -unit_key
    insert_dir = unit_key * learn_rate

    def split_time(values_in):
        return jnp.swapaxes(values_in.reshape(blocks, SUB, head_count, HEAD_SIZE), 0, 1)

    series = tuple(
        (
            split_time(member)
            for member in (
                decay_rate,
                keys_single,
                values_single,
                remove_dir,
                insert_dir,
                receptance_rows,
            )
        )
    )
    head_eye = jnp.broadcast_to(
        jnp.eye(HEAD_SIZE, dtype=jnp.float32), (head_count, HEAD_SIZE, HEAD_SIZE)
    )
    block_eye = jnp.broadcast_to(head_eye[None], (blocks, head_count, HEAD_SIZE, HEAD_SIZE))

    def advance(current, inputs):
        product, memory = current
        decay_t, key_t, value_t, remove_t, insert_t, recept_t = inputs
        shifted = jnp.einsum("bhij,bhj->bhi", product, remove_t, precision=EXACT)
        product = product * decay_t[:, :, None, :] + shifted[..., None] * insert_t[:, :, None, :]
        erased = jnp.einsum("bhij,bhj->bhi", memory, remove_t, precision=EXACT)
        memory = (
            memory * decay_t[:, :, None, :]
            + erased[..., None] * insert_t[:, :, None, :]
            + value_t[..., None] * key_t[:, :, None, :]
        )
        seen_part = jnp.einsum("bhij,bhj->bhi", product, recept_t, precision=EXACT)
        local_part = jnp.einsum("bhij,bhj->bhi", memory, recept_t, precision=EXACT)
        return ((product, memory), (seen_part, local_part))

    (block_prod, block_state), (seen_part, local_part) = lax.scan(
        advance, (block_eye, jnp.zeros_like(block_eye)), series
    )
    inclusive = lax.associative_scan(compose, (block_prod, block_state), axis=0)
    before_prod = jnp.concatenate([head_eye[None], inclusive[0][:-1]], axis=0)
    before_state = jnp.concatenate([jnp.zeros_like(head_eye)[None], inclusive[1][:-1]], axis=0)
    totals = (inclusive[0][-1], inclusive[1][-1])
    incoming = entering(totals, SP, compose, (head_eye, jnp.zeros_like(head_eye)))[1]
    entry_state = (
        jnp.einsum("hij,bhjk->bhik", incoming, before_prod, precision=EXACT) + before_state
    )
    joined = jnp.einsum("bhij,tbhj->tbhi", entry_state, seen_part, precision=EXACT) + local_part
    recurrence_output = jnp.swapaxes(joined, 0, 1).reshape(layout)
    mixer_output = final_output(
        recurrence_output,
        receptance_rows,
        keys_single,
        values_single,
        self_token_weight,
        head_norm_gain,
        output_gate_preact,
    )
    own_rows = sequence_length // lax.axis_size("tp")
    row_start = lax.axis_index("tp") * own_rows
    mix_sum = summed_on_arrival(
        jnp.dot(mixer_output, output_weight, preferred_element_type=jnp.float32).astype(
            jnp.bfloat16
        ),
        "tp",
        0,
    )
    mix = lax.optimization_barrier(mix_sum.astype(jnp.bfloat16)).astype(jnp.float32)
    resid_rows = lax.dynamic_slice_in_dim(residual, row_start, own_rows, 0)
    after_mix = (resid_rows.astype(jnp.float32) + mix).astype(jnp.bfloat16)
    normed = gather_directly(rms_scale(after_mix, premixer_norm_gain), "tp", 0)
    pieces = sent_together((mixer_gate_weight, mixer_up_weight), SP, 0, 1)
    gate_more = jnp.dot(normed, pieces[0], preferred_element_type=jnp.float32)
    up_more = jnp.dot(normed, pieces[1], preferred_element_type=jnp.float32)
    hidden = (jax.nn.silu(gate_more) * up_more).astype(jnp.bfloat16)
    down_full = gather_axes(mixer_down_weight, SP, 1)
    down_sum = summed_on_arrival(
        jnp.dot(hidden, down_full, preferred_element_type=jnp.float32).astype(jnp.bfloat16), "tp", 0
    )
    return (after_mix.astype(jnp.float32) + down_sum).astype(jnp.bfloat16)


def solution(mesh):
    torus = Mesh(mesh.devices.reshape(16, 4, mesh.shape["tp"]), ("sp_0", "sp_1", "tp"))
    in_specs = (
        P(SP, "tp"),
        P(SP, "tp"),
        P(SP, "tp"),
        P(SP, "tp"),
        P(SP, "tp"),
        P(SP, "tp"),
        P("tp", None),
        P("tp"),
        P("tp", None),
        P(SP, None),
        P(),
        P(SP, "tp"),
        P(SP, "tp"),
        P("tp", SP),
    )
    out_specs = P(SP_TP, None)
    return jax.shard_map(
        per_device, mesh=torus, in_specs=in_specs, out_specs=out_specs, check_vma=False
    )
```

profile of v0, /device:TPU:1, one launch (start us, length us, event | category | flops | bytes accessed | tf_op | source)
XLA Modules:
  0.0 540.6 jit_solution(4914291655720536326)
XLA Ops:
  12.4 150.7 %while.17 = (s32[]{:T(128)}, f32[12,2,64,64]{3,2,1,0:T(8,128)S(1)}, f32[12,2,64,64]{3,2,1,0:T(8,128)S(1)}, f32[16,12,2,64]{3,0,2,1:T(8,128)}, f32[16,12,2,64]{3,...) while((s32[]{:T(128)}, f32[12,2,64,64]{3,2,1,0:T(8,128)S(1)}, ...), condition=%wide.region_2.3_spmd.clone, body=%wide.region_1.2_spmd.clone.sunk | while | flops 5701635 | bytes 3330204 | solution.py:200
  20.2 1.6 dynamic_update_slice.11
  29.6 1.6 dynamic_update_slice.11
  48.5 1.6 dynamic_update_slice.11
  57.9 1.6 dynamic_update_slice.11
  168.7 2.6 pad.48
  171.3 2.6 pad.47
  176.3 4.6 pad.50
  181.7 2.6 pad.42
  184.3 2.7 pad.41
  187.0 4.6 pad.49
  192.8 4.6 pad.104
  199.1 11.2 %all-gather = f32[1024,64]{1,0:T(8,128)S(1)} all-gather(f32[256,64]{1,0:T(8,128)S(1)} %pad_maximum_fusion.6), channel_id=2, replica_groups=mesh['sp_0'=16,'sp_1'=4,'tp'=8] {'sp_1'}, dimensions={0}, use_global_device_ids=true | all-gather | bytes 327680 | tf_op jit(solution)/shard_map/all_gather | solution.py:32
  214.3 11.2 %all_gather.26 = bf16[640,128]{0,1:T(8,128)(2,1)} all-gather(bf16[640,32]{0,1:T(8,128)(2,1)} %param.29), channel_id=1, replica_groups=mesh['sp_0'=16,'sp_1'=4,'tp'=8] {'sp_1'}, dimensions={1}, use_global_device_ids=true | all-gather | bytes 204800 | tf_op jit(solution)/shard_map/all_gather | solution.py:94
  225.6 4.6 pad.73
  237.3 45.9 %all-gather.10.cloned.1.call-done = f32[4096,64]{1,0:T(8,128)} async-done(((f32[256,64]{1,0:T(8,128)}), f32[4096,64]{1,0:T(8,128)}) %all-gather.10.cloned.1.call-update) | async-done | bytes 1048592 | tf_op jit(solution)/shard_map/all_gather | solution.py:32
  294.3 14.6 %all-to-all-start = ((bf16[8,24,2048]{2,1,0:T(8,128)(2,1)}), bf16[8,24,2048]{2,1,0:T(8,128)(2,1)S(1)}, u32[]{:S(2)}, u32[]{:S(2)}) async-start(bf16[8,24,2048]{2,1,0:T(8,128)(2,1)} %bitcast.71), calls=%async_computation | async-start | bytes 1572864 | tf_op jit(solution)/shard_map/all_to_all | solution.py:64
  308.8 12.2 %all-to-all-done = bf16[8,24,2048]{2,1,0:T(8,128)(2,1)S(1)} async-done(((bf16[8,24,2048]{2,1,0:T(8,128)(2,1)}), bf16[8,24,2048]{2,1,0:T(8,128)(2,1)S(1)}, u32[]{:S(2)}, u32[]{:S(2)}) %all-to-all-start) | async-done | bytes 786464 | tf_op jit(solution)/shard_map/all_to_all | solution.py:64
  322.4 15.5 %all_to_all.15 = bf16[8,24,2048]{2,1,0:T(8,128)(2,1)S(1)} all-to-all(bf16[8,24,2048]{2,1,0:T(8,128)(2,1)S(1)} %broadcast_in_dim.45), channel_id=1, replica_groups=mesh['sp_0'=16,'sp_1'=4,'tp'=8] {'tp'}, dimensions={0} | all-to-all | bytes 1572864 | tf_op jit(solution)/shard_map/all_to_all | solution.py:76
  337.9 94.2 %all-gather.6.cloned.1.call-done = bf16[2048,1280]{1,0:T(8,128)(2,1)} async-done(((bf16[32,1280]{1,0:T(8,128)(2,1)}), bf16[2048,1280]{1,0:T(8,128)(2,1)}) %all-gather.6.cloned.1.call-update) | async-done | bytes 5242896 | tf_op jit(solution)/shard_map/all_gather | solution.py:85
  432.1 2.5 fusion.8
  434.6 68.1 %all-gather.8.cloned.1.call-done = bf16[640,2048]{0,1:T(8,128)(2,1)} async-done(((bf16[640,128]{0,1:T(8,128)(2,1)}), bf16[640,2048]{0,1:T(8,128)(2,1)}) %all-gather.8.cloned.1.call-update) | async-done | bytes 2621456 | tf_op jit(solution)/shard_map/all_gather | solution.py:94
  502.7 4.2 convolution_convert_fusion
  506.9 26.3 %all_to_all.16 = bf16[8,24,2048]{2,1,0:T(8,128)(2,1)S(1)} all-to-all(bf16[8,24,2048]{2,1,0:T(8,128)(2,1)S(1)} %bitcast.263), channel_id=1, replica_groups=mesh['sp_0'=16,'sp_1'=4,'tp'=8] {'tp'}, dimensions={0} | all-to-all | bytes 1572864 | tf_op jit(solution)/shard_map/all_to_all | solution.py:64
  (321 shorter events, 184.5 us)
Async XLA Ops:
  6.5 286.4 %copy-start = (bf16[128,2048]{1,0:T(8,128)(2,1)S(1)}, bf16[128,2048]{1,0:T(8,128)(2,1)}, u32[]{:S(2)}) copy-start(bf16[128,2048]{1,0:T(8,128)(2,1)} %param.24) | copy-start | bytes 1572868
  6.5 5.3 copy-start.18
  6.5 5.6 %copy-start.17 = (bf16[192,128]{1,0:T(8,128)(2,1)S(1)}, bf16[192,128]{1,0:T(8,128)(2,1)}, u32[]{:S(2)}) copy-start(bf16[192,128]{1,0:T(8,128)(2,1)} %param.18) | copy-start | bytes 147460
  6.5 276.6 %all-gather.10.cloned.1.call-start = ((), (), s32[]{:S(2)}) async-start(), calls=%async_computation.5 | async-start | bytes 2228224 | tf_op jit(solution)/shard_map/all_gather | solution.py:32
  181.3 5.7 %copy-start.5 = (f32[5,2,64,64]{3,2,1,0:T(8,128)S(1)}, f32[5,2,64,64]{3,2,1,0:T(8,128)}, u32[]{:S(2)}) copy-start(f32[5,2,64,64]{3,2,1,0:T(8,128)} %convolution_add_fusion.1) | copy-start | bytes 491524
  184.3 13.9 %copy-start.1 = (f32[12,2,64,64]{3,2,1,0:T(8,128)S(1)}, f32[12,2,64,64]{3,2,1,0:T(8,128)}, u32[]{:S(2)}) copy-start(f32[12,2,64,64]{3,2,1,0:T(8,128)} %pad.50) | copy-start | bytes 1179652
  211.4 14.2 %copy-start.6 = (f32[2,64,64]{2,1,0:T(8,128)}, f32[2,64,64]{2,1,0:T(8,128)S(1)}, u32[]{:S(2)}) copy-start(f32[2,64,64]{2,1,0:T(8,128)S(1)} %fusion.108) | copy-start | bytes 98308
  211.6 14.0 %copy-start.8 = (f32[2,64,64]{2,1,0:T(8,128)}, f32[2,64,64]{2,1,0:T(8,128)S(1)}, u32[]{:S(2)}) copy-start(f32[2,64,64]{2,1,0:T(8,128)S(1)} %convolution_add_fusion.23) | copy-start | bytes 98308
  211.8 13.8 %copy-start.10 = (f32[2,64,64]{2,1,0:T(8,128)}, f32[2,64,64]{2,1,0:T(8,128)S(1)}, u32[]{:S(2)}) copy-start(f32[2,64,64]{2,1,0:T(8,128)S(1)} %convolution_add_fusion.22) | copy-start | bytes 98308
  212.0 13.6 %copy-start.12 = (f32[2,64,64]{2,1,0:T(8,128)}, f32[2,64,64]{2,1,0:T(8,128)S(1)}, u32[]{:S(2)}) copy-start(f32[2,64,64]{2,1,0:T(8,128)S(1)} %convolution_add_fusion.21) | copy-start | bytes 98308
  212.7 219.4 %all-gather.6.cloned.1.call-start = ((), (), s32[]{:S(2)}) async-start(), calls=%async_computation.3 | async-start | bytes 5324800 | tf_op jit(solution)/shard_map/all_gather | solution.py:85
  214.2 288.5 %all-gather.8.cloned.1.call-start = ((), (), s32[]{:S(2)}) async-start(), calls=%async_computation.4 | async-start | bytes 2785280 | tf_op jit(solution)/shard_map/all_gather | solution.py:94
  233.1 4.0 copy-start.7
  286.0 3.3 copy-start.9
  286.0 3.3 copy-start.11
  286.0 3.3 copy-start.13
  286.4 3.1 copy-start.3
  288.0 2.4 copy-start.15
  288.1 2.4 copy-start.16
  289.5 3.4 copy-start.14
  289.6 3.3 copy-start.19
  289.6 3.3 copy-start.21
  292.6 29.6 %copy-start.20 = (f32[2048]{0:T(1024)S(1)}, f32[2048]{0:T(1024)}, u32[]{:S(2)}) copy-start(f32[2048]{0:T(1024)} %param.26) | copy-start | bytes 24580
  294.3 26.7 %all-to-all-start = ((bf16[8,24,2048]{2,1,0:T(8,128)(2,1)}), bf16[8,24,2048]{2,1,0:T(8,128)(2,1)S(1)}, u32[]{:S(2)}, u32[]{:S(2)}) async-start(bf16[8,24,2048]{2,1,0:T(8,128)(2,1)} %bitcast.71), calls=%async_computation | async-start | bytes 1572864 | tf_op jit(solution)/shard_map/all_to_all | solution.py:64
  (2 other events, 3.8 us)
Sparse Core Ops, SparseCore 0:
  212.8 70.3 all-gather.9
  286.1 145.9 all-gather.5
  434.2 68.4 all-gather.7
where the time goes:
time: 543 us; the launch traced here: 541 us
  waiting for transfers between devices  220 us (41%)
  matrix products  107 us (20%)
  local copies, waits for them, and re-layouts  92.3 us (17%)
  blocking collectives  64.3 us (12%)
  other arithmetic  27.2 us (5%)
  starting transfers between devices  14.7 us (3%)
  between operations  14.1 us (3%)
    all_gather x1, waiting for transfers between devices, sent_together(): out, at, done = (lax.all_gather(both, axis, axis=dim, tiled=True), 0, [])  94.2 us
    all_gather x1, waiting for transfers between devices, gather_axes(): x = lax.all_gather(x, axis, axis=dim, tiled=True)  68.1 us
    dynamic_update_slice x32, local copies, waits for them, and re-layouts, per_device(): lax.scan(advance, (block_eye, jnp.zeros_like(block_eye)), series)  51.1 us
    all_gather x1, waiting for transfers between devices, gathered_once(): both, at, found = (lax.all_gather(jnp.concatenate(lines), axis), 0, {})  45.9 us
    all_to_all x1, blocking collectives, summed_on_arrival(): tiles = lax.all_to_all(split_up(x, dim, length), axis, 0, 0, tiled=True)  26.3 us
    pad x10, local copies, waits for them, and re-layouts, per_device(): inclusive = lax.associative_scan(compose, (block_prod, block_state), axis=0)  21.7 us
    dot_general x16, matrix products, advance(): shifted = jnp.einsum('bhij,bhj->bhi', product, remove_t, precision=EXACT)  21.5 us
    dot_general x16, matrix products, advance(): erased = jnp.einsum('bhij,bhj->bhi', memory, remove_t, precision=EXACT)  21.4 us
  transfers between devices with their start and end apart: 4, of which 4 were waited for; matrix products, arithmetic and copies ran while one was open for 5% of the time, Pallas kernels for 0%

commit v1 on v0

v1 whole, which is shorter than its diff:
```python
import functools
import math

import jax
import jax.numpy as jnp
from jax import lax
from jax.experimental import pallas as pl
from jax.experimental.pallas import tpu as pltpu
from jax.sharding import Mesh
from jax.sharding import PartitionSpec as P

F32, BF16 = jnp.float32, jnp.bfloat16
EXACT = lax.Precision.HIGHEST
MESH = pl.DeviceIdType.MESH
GROUP_EPS = 0.00064
NORM_EPS = 1e-06

NZ, NY, NX, NC = 16, 4, 4, 2
N = 192
ROWS = 24
D = 2048
FF = 640
W = 32


def dot(a, b, ca=1, cb=0):
    return lax.dot_general(
        a.astype(BF16), b.astype(BF16), (((ca,), (cb,)), ((), ())), preferred_element_type=F32
    )


def dotx(a, b, ca=1, cb=0):
    return lax.dot_general(
        a, b, (((ca,), (cb,)), ((), ())), precision=EXACT, preferred_element_type=F32
    )


def iota(shape, d):
    return lax.broadcasted_iota(jnp.int32, shape, d)


def head_ones():
    return jnp.where(iota((128, 128), 0) // 64 == iota((128, 128), 1) // 64, 1.0, 0.0).astype(F32)


def invert(low):
    n = low.shape[0]
    row, col = iota((n, n), 0), iota((n, n), 1)
    eye = jnp.where(row == col, 1.0, 0.0).astype(F32)
    d = jnp.where(row // 8 == col // 8, low, 0.0)
    d2 = dotx(d, d)
    d4 = dotx(d2, d2)
    x = eye + d
    x = x + dotx(d2, x)
    x = x + dotx(d4, x)
    m = 8
    while m < 64:
        off = jnp.where((row // (2 * m) == col // (2 * m)) & (row // m != col // m), low, 0.0)
        x = x + dot(x, dot(off, x))
        m *= 2
    off = jnp.where(row // 64 != col // 64, low, 0.0)
    y = dot(x, off)
    z = dot(y, x)
    return x + z + dot(y, z)


def local_scan(r, k, v, dec, lr, service):
    r, k, v = r.astype(F32), k.astype(F32), v.astype(F32)
    lw = (-math.exp(-0.5)) / (1.0 + jnp.exp(-dec))
    row, col = iota((N, N), 0), iota((N, N), 1)
    c = dotx(jnp.where(row >= col, 1.0, 0.0).astype(F32), lw)
    norm = jnp.sqrt(dotx(k * k, head_ones()))
    unit = k / jnp.maximum(norm, 1.0)
    ins = unit / (1.0 + jnp.exp(-lr))
    up, dn = jnp.exp(c), jnp.exp(-c)
    last = c[N - 1 : N]
    rest = jnp.exp(last - c)
    at = -unit * jnp.exp(c - lw)
    rt = r * up
    left = jnp.concatenate([at, rt], 0)
    right = jnp.concatenate([ins * dn, k * dn], 0).astype(BF16)
    lane2 = iota((N, 256), 1) % 128
    us, outs = [], []
    for h in range(2):
        head_lanes = iota((2 * N, 128), 1) // 64 == h
        g = dot(jnp.where(head_lanes, left, 0.0), right, 1, 1)
        low = jnp.where(row > col, g[:N, :N], 0.0)
        mak = jnp.where(row > col, g[:N, N:], 0.0)
        mrb = jnp.where(row >= col, g[N:, :N], 0.0)
        mrk = jnp.where(row >= col, g[N:, N:], 0.0)
        x = invert(low)
        u = dot(x, jnp.concatenate([at, dot(mak, v)], 1))
        o = dot(mrb, u)
        ov = dot(mrk, v)
        us.append(u)
        outs.append(jnp.concatenate([o[:, :128] + rt, o[:, 128:] + ov], 1))
        service()
    u = jnp.where(lane2 < 64, us[0], us[1])
    o = jnp.where(lane2 < 64, outs[0], outs[1])
    f = dot((ins * rest).T, u)
    fl = f[:, 128:] + dot((k * rest).T, v)
    ones = head_ones()
    r1, c1 = iota((128, 128), 0), iota((128, 128), 1)
    e = f[:, :128] * ones + jnp.where(r1 == c1, jnp.exp(last) - 1.0, 0.0)
    l = fl * ones
    return e[:64] + e[64:], l[:64] + l[64:], o


def unpack(p):
    first = iota(p.shape, 1) % 128 < 64
    return jnp.concatenate([jnp.where(first, p, 0.0), jnp.where(first, 0.0, p)], 0)


def pack(p):
    first = iota((64, p.shape[1]), 1) % 128 < 64
    return jnp.where(first, p[:64], p[64:])


def kernel(
    r_ref, k_ref, v_ref, dec_ref, lr_ref, og_ref, stw_ref, hng_ref, wo_ref, res_ref, png_ref,
    wg_ref, wu_ref, wd_ref,
    out_ref,
    gu, dn, state, entry_buf, part, pair_in, mine, mix_in, rows_buf, nrm, local_out, resid,
    loc_sem, zs, zr, ys, yr, as_, ar, azs, azr, ss, sr, ps, pr, xs, xr, gs, gr, fs, fr,
):
    z, y, x, core = (lax.axis_index(a) for a in ("z", "y", "x", "c"))
    here = z * NY + y

    def at(dz=0, dy=0, dx=0, dc=0):
        return (
            lax.rem(z + dz + NZ, NZ), lax.rem(y + dy + NY, NY),
            lax.rem(x + dx + NX, NX), lax.rem(core + dc, NC),
        )

    sends = []

    def push(src, dst, send, recv, to):
        cp = pltpu.make_async_remote_copy(
            src_ref=src, dst_ref=dst, send_sem=send, recv_sem=recv, device_id=to,
            device_id_type=MESH,
        )
        cp.start()
        sends.append(cp)
        return cp

    def landed(dst, send, recv):
        pltpu.make_async_remote_copy(
            src_ref=dst, dst_ref=dst, send_sem=send, recv_sem=recv, device_id=at(dz=1),
            device_id_type=MESH,
        ).wait_recv()

    own = [
        pltpu.make_async_copy(wg_ref, gu.at[here, pl.ds(0, W)], loc_sem.at[0]),
        pltpu.make_async_copy(wu_ref, gu.at[here, pl.ds(W, W)], loc_sem.at[1]),
        pltpu.make_async_copy(wd_ref, dn.at[here], loc_sem.at[2]),
    ]
    row0 = pl.multiple_of((x * NC + core) * ROWS, 8)
    fetch = pltpu.make_async_copy(res_ref.at[pl.ds(row0, ROWS)], resid, loc_sem.at[3])
    for cp in own:
        cp.start()
    fetch.start()

    zb, za = z % 4, z // 4
    peers = [at(dz=1), at(dz=-1), at(dy=1), at(dy=2), at(dy=3)]
    peers += [at(dx=d) for d in (1, 2, 3)] + [at(dc=1)]
    z_near = [(za * 4 + lax.rem(zb + d, 4), y, x, core) for d in (1, 2, 3)]
    z_far = [at(dz=4 * d) for d in (1, 2, 3)]
    peers += z_near + z_far
    barrier = pltpu.get_barrier_semaphore()
    for p in peers:
        pl.semaphore_signal(barrier, inc=1, device_id=p, device_id_type=MESH)
    for cp in own:
        cp.wait()
    pl.semaphore_wait(barrier, len(peers))

    def slot(dz, dy=0):
        return lax.rem(z + dz + NZ, NZ) * NY + lax.rem(y + dy + NY, NY)

    def column(dz):
        return pl.multiple_of(lax.rem(z + dz + NZ, NZ) * NY, NY)

    def offsets(s):
        return [0] if s == 0 else ([-s, s] if s < 8 else [8])

    def index(o):
        return 0 if o == 0 else (15 if o == 8 else 2 * abs(o) - (1 if o < 0 else 0))

    def y_out(o):
        i = index(o)
        src = gu.at[slot(o)]
        push(src, src, ys.at[i, 0], yr.at[i, 0], at(dy=1))
        push(src, src, ys.at[i, 1], yr.at[i, 1], at(dy=-1))

    def y_on(o):
        i = index(o)
        a, b = gu.at[slot(o, -1)], gu.at[slot(o, 1)]
        landed(a, ys.at[i, 0], yr.at[i, 0])
        a = gu.at[slot(o, -1), pl.ds(0, W)]
        push(a, a, ys.at[i, 2], yr.at[i, 2], at(dy=1))
        landed(b, ys.at[i, 1], yr.at[i, 1])
        b = gu.at[slot(o, 1), pl.ds(W, W)]
        push(b, b, ys.at[i, 3], yr.at[i, 3], at(dy=-1))

    def y_end(o):
        i = index(o)
        landed(gu.at[slot(o, 2), pl.ds(0, W)], ys.at[i, 2], yr.at[i, 2])
        landed(gu.at[slot(o, 2), pl.ds(W, W)], ys.at[i, 3], yr.at[i, 3])

    def z_block(dz, d, s):
        b = gu.at[slot(dz)]
        return b if s < 8 else gu.at[slot(dz), pl.ds(W * d, W)]

    def z_out(s):
        for d in range(2):
            o = -s if d == 0 else s
            b = z_block(o, d, s + 1)
            push(b, b, zs.at[d, s], zr.at[d, s], at(dz=1 if d == 0 else -1))

    def z_in(s):
        for d in range(2):
            landed(z_block(-s if d == 0 else s, d, s), zs.at[d, s - 1], zr.at[d, s - 1])

    def a_block(dz, d, s):
        return dn.at[pl.ds(column(dz), NY)] if s < 8 else dn.at[pl.ds(column(dz) + 2 * d, 2)]

    def a_out(s):
        for d in range(2):
            b = a_block(-s if d == 0 else s, d, s + 1)
            push(b, b, azs.at[d, s], azr.at[d, s], at(dz=1 if d == 0 else -1))

    def a_in(s):
        for d in range(2):
            b = a_block(-s if d == 0 else s, d, s)
            landed(b, azs.at[d, s - 1], azr.at[d, s - 1])

    turn = [0]

    def service():
        s = turn[0]
        turn[0] += 1
        if s == 0:
            z_out(0)
            for d in (1, 2, 3):
                push(dn.at[here], dn.at[here], as_.at[d - 1], ar.at[d - 1], at(dy=d))
            y_out(0)
        elif s <= 8:
            z_in(s)
            if s < 8:
                z_out(s)
            if s == 1:
                for d in (1, 2, 3):
                    landed(dn.at[slot(0, -d)], as_.at[d - 1], ar.at[d - 1])
            else:
                a_in(s - 1)
            a_out(s - 1)
            for o in offsets(s):
                y_out(o)
            for o in offsets(s - 1):
                y_on(o)
        elif s == 9:
            a_in(8)
            for o in offsets(8):
                y_on(o)
            for t in range(9):
                for o in offsets(t):
                    y_end(o)

    service()

    e, l, o = local_scan(r_ref[...], k_ref[...], v_ref[...], dec_ref[...], lr_ref[...], service)
    local_out[...] = o

    def level(n, x_own, mates, place):
        state[n, place, :, :128] = x_own[0].astype(BF16)
        state[n, place, :, 128:] = x_own[1].astype(BF16)
        for d in (1, 2, 3):
            b = state.at[n, place]
            push(b, b, ss.at[n, d - 1], sr.at[n, d - 1], mates[d - 1])
        for d in (1, 2, 3):
            landed(state.at[n, lax.rem(place - d + 4, 4)], ss.at[n, d - 1], sr.at[n, d - 1])
        total = unpack(state[n, 0].astype(F32))
        before = jnp.zeros_like(total)
        for j in range(1, 4):
            before = jnp.where(place == j, total, before)
            nxt = unpack(state[n, j].astype(F32))
            total = total + nxt + dot(nxt[:, :128], total)
        return total, before

    y_mates = [at(dy=d) for d in (1, 2, 3)]
    t1, b1 = level(0, (e, l), y_mates, y)
    service()
    p1 = pack(t1)
    t2, b2 = level(1, (p1[:, :128], p1[:, 128:]), z_near, zb)
    service()
    p2 = pack(t2)
    _, b3 = level(2, (p2[:, :128], p2[:, 128:]), z_far, za)
    h0 = b3[:, 128:]
    h0 = h0 + dot(b2[:, :128], h0) + b2[:, 128:]
    h0 = h0 + dot(b1[:, :128], h0) + b1[:, 128:]

    o = local_out[...]
    mech = dot(o[:, :128], h0) + o[:, 128:]
    ones = head_ones()
    rf, kf, vf = r_ref[...].astype(F32), k_ref[...].astype(F32), v_ref[...].astype(F32)
    centred = mech - dotx(mech, ones) * (1.0 / 64)
    spread = dotx(centred * centred, ones) * (1.0 / 64)
    token = dotx(rf * kf * stw_ref[...], ones) * vf
    mixed = centred * lax.rsqrt(spread + GROUP_EPS) * hng_ref[...] + token
    mixed = (mixed / (1.0 + jnp.exp(-og_ref[...].astype(F32)))).astype(BF16)

    def shares(a, b, cb):
        for j in range(4):
            cols = D // 4 * j
            bj = b[:, cols : cols + D // 4] if cb == 0 else b[cols : cols + D // 4]
            prod = dot(a, bj, 1, cb)
            for p in range(8):
                part[p // 2, p % 2, :, cols : cols + D // 4] = prod[
                    p * ROWS : (p + 1) * ROWS
                ].astype(BF16)

    def scattered_sum(n):
        other = 1 - core
        for j in range(4):
            push(part.at[j, other], pair_in.at[n, j], ps.at[n, j], pr.at[n, j], at(dc=1))
        for d in (2, 1, 3, 0):
            j = lax.rem(x + d, NX)
            landed(pair_in.at[n, j], ps.at[n, j], pr.at[n, j])
            mine[n, j] = (part[j, core].astype(F32) + pair_in[n, j].astype(F32)).astype(BF16)
            if d:
                push(mine.at[n, j], mix_in.at[n, d - 1], xs.at[n, d - 1], xr.at[n, d - 1], at(dx=d))
        total = mine[n, x].astype(F32)
        for d in (1, 3, 2):
            landed(mix_in.at[n, d - 1], xs.at[n, d - 1], xr.at[n, d - 1])
            total = total + mix_in[n, d - 1].astype(F32)
        return total

    def finish_sends():
        for cp in sends:
            cp.wait_send()
        sends.clear()

    shares(mixed, wo_ref[...], 0)
    service()
    mix = scattered_sum(0).astype(BF16).astype(F32)
    service()
    fetch.wait()
    after = (resid[...].astype(F32) + mix).astype(BF16).astype(F32)
    factor = lax.rsqrt(jnp.mean(after * after, axis=-1, keepdims=True) + NORM_EPS)
    normed = (after * factor * png_ref[...]).astype(BF16)

    rows_buf[x, core] = normed
    mine_rows = rows_buf.at[x, core]
    push(mine_rows, mine_rows, gs.at[0], gr.at[0], at(dc=1))
    for d in (2, 1, 3):
        push(mine_rows, mine_rows, gs.at[d], gr.at[d], at(dx=d))
    for d in (1, 3, 2):
        b = rows_buf.at[lax.rem(x + NX - d, NX), core]
        landed(b, gs.at[d], gr.at[d])
        push(b, b, fs.at[d - 1], fr.at[d - 1], at(dc=1))
    service()
    landed(rows_buf.at[x, 1 - core], gs.at[0], gr.at[0])
    for d in (1, 3, 2):
        b = rows_buf.at[lax.rem(x + NX - d, NX), 1 - core]
        landed(b, fs.at[d - 1], fr.at[d - 1])
    for j in range(8):
        nrm[j * ROWS : (j + 1) * ROWS] = rows_buf[j // 2, j % 2]
    while turn[0] <= 9:
        service()
    finish_sends()

    gate = jnp.zeros((N, FF), F32)
    upper = jnp.zeros((N, FF), F32)
    for j in range(8):
        a = nrm[:, j * 256 : (j + 1) * 256]
        gate = gate + dot(a, gu[j * 8 : (j + 1) * 8, :W].reshape(256, FF))
        upper = upper + dot(a, gu[j * 8 : (j + 1) * 8, W:].reshape(256, FF))
    hidden = (gate / (1.0 + jnp.exp(-gate)) * upper).astype(BF16)
    shares(hidden, dn[...].reshape(D, FF), 1)
    down = scattered_sum(1)
    out_ref[...] = (after + down).astype(BF16)
    finish_sends()


def per_device(r, k, v, dec, lr, og, stw, hng, wo, res, png, wg, wu, wd):
    vmem = pl.BlockSpec(memory_space=pltpu.VMEM)
    hbm = pl.BlockSpec(memory_space=pl.ANY)
    dma = pltpu.SemaphoreType.DMA
    return pl.pallas_call(
        kernel,
        out_shape=jax.ShapeDtypeStruct((ROWS, D), BF16),
        in_specs=[vmem] * 9 + [hbm] + [vmem] + [hbm] * 3,
        out_specs=vmem,
        scratch_shapes=[
            pltpu.VMEM((64, 2 * W, FF), BF16),
            pltpu.VMEM((64, W, FF), BF16),
            pltpu.VMEM((3, 4, 64, 256), BF16),
            pltpu.VMEM((8, 128), F32),
            pltpu.VMEM((NX, NC, ROWS, D), BF16),
            pltpu.VMEM((2, NX, ROWS, D), BF16),
            pltpu.VMEM((2, NX, ROWS, D), BF16),
            pltpu.VMEM((2, 3, ROWS, D), BF16),
            pltpu.VMEM((NX, NC, ROWS, D), BF16),
            pltpu.VMEM((N, D), BF16),
            pltpu.VMEM((N, 256), F32),
            pltpu.VMEM((ROWS, D), BF16),
            dma((4,)),
            dma((2, 8)), dma((2, 8)),
            dma((16, 4)), dma((16, 4)),
            dma((3,)), dma((3,)),
            dma((2, 8)), dma((2, 8)),
            dma((3, 3)), dma((3, 3)),
            dma((2, 4)), dma((2, 4)),
            dma((2, 3)), dma((2, 3)),
            dma((4,)), dma((4,)),
            dma((3,)), dma((3,)),
        ],
        compiler_params=pltpu.CompilerParams(
            collective_id=0, has_side_effects=True, vmem_limit_bytes=60 * 1024 * 1024
        ),
        name="layer",
    )(r, k, v, dec, lr, og, stw.reshape(1, 128), hng.reshape(1, 128), wo, res,
      png.reshape(1, D), wg, wu, wd.T)


def solution(mesh):
    torus = Mesh(mesh.devices.reshape(NZ, NY, NX, NC), ("z", "y", "x", "c"))
    sp, tp = ("z", "y"), ("x", "c")
    seq = P(sp, tp)
    return jax.shard_map(
        per_device,
        mesh=torus,
        in_specs=(
            seq, seq, seq, seq, seq, seq, P(tp, None), P(tp), P(tp, None), P(sp, None), P(),
            seq, seq, P(tp, sp),
        ),
        out_specs=P((*sp, *tp), None),
        check_vma=False,
    )
```

time: 543 us -> 107 us (0.20)
  waiting for transfers between devices: 220 us -> 0 us
  matrix products: 107 us -> 0 us
  Pallas kernels: 0 us -> 104 us
  local copies, waits for them, and re-layouts: 92.3 us -> 2.81 us
  blocking collectives: 64.3 us -> 0 us
  other arithmetic: 27.2 us -> 0 us
  starting transfers between devices: 14.7 us -> 0 us
  between operations: 14.1 us -> 0.01 us
    all_gather x3 -> x0, waiting for transfers between devices: 208 us -> none  [the longest x1 94.2 us: sent_together(): out, at, done = (lax.all_gather(both, axis, axis=dim, tiled=True), 0, [])]
    dot_general x108 -> x0, matrix products: 107 us -> none  [the longest x16 21.5 us: advance(): shifted = jnp.einsum('bhij,bhj->bhi', product, remove_t, precision=EXACT)]
    pallas_call x0 -> x1, Pallas kernels: none -> 104 us  [per_device(): pl.pallas_call(kernel, out_shape=jax.ShapeDtypeStruct((ROWS, D), BF16), i...]
    dynamic_update_slice x32 -> x0, local copies, waits for them, and re-layouts: 51.1 us -> none  [per_device(): lax.scan(advance, (block_eye, jnp.zeros_like(block_eye)), series)]
    all_to_all x2 -> x0, blocking collectives: 41.9 us -> none  [the longest x1 26.3 us: summed_on_arrival(): tiles = lax.all_to_all(split_up(x, dim, length), axis, 0, 0, tiled=True)]
    all_gather x2 -> x0, blocking collectives: 22.5 us -> none  [the longest x1 11.2 us: gathered_once(): both, at, found = (lax.all_gather(jnp.concatenate(lines), axis), 0, {})]
    pad x10 -> x0, local copies, waits for them, and re-layouts: 21.7 us -> none  [per_device(): inclusive = lax.associative_scan(compose, (block_prod, block_state), axis=0)]
    add x23 -> x0, other arithmetic: 17.1 us -> none  [the longest x16 12.9 us: advance(): memory * decay_t[:, :, None, :]]
  transfers between devices with their start and end apart: 4 -> 0, of which waited for: 4 -> 0; matrix products, arithmetic and copies ran while one was open for 5% -> 0% of each run, Pallas kernels for 0% -> 0%
where the time goes in v1:
time: 107 us; the launch traced here: 106 us
  Pallas kernels  104 us (97%)
  local copies, waits for them, and re-layouts  2.81 us (3%)
    pallas_call x1, Pallas kernels, per_device(): pl.pallas_call(kernel, out_shape=jax.ShapeDtypeStruct((ROWS, D), BF16), i...  104 us
    unnamed x3, local copies, waits for them, and re-layouts  2.22 us

profile of v1, /device:TPU:1, one launch (start us, length us, event | category | flops | bytes accessed | tf_op | source)
XLA Modules:
  0.0 106.4 jit_solution(3915399818146004772)
XLA Ops:
  0.0 0.0 copy-start
  0.0 0.7 copy-done
  0.7 0.6 reshape.9.stw_ref
  1.3 103.6 %layer.1 = bf16[24,2048]{1,0:T(8,128)(2,1)} custom-call(bf16[192,128]{1,0:T(8,128)(2,1)} %r_ref.1, bf16[192,128]{1,0:T(8,128)(2,1)} %k_ref.1, bf16[192,128]{1,0:T(8,128)(2,1)} %v_ref.1, f32[192,128]{1,0:T(8,128)} %dec_ref.1, f32[192,128]{1,0:T(8,128)} %lr_ref.1, bf16[192,128]{1,0:T(8,128)(2,1)} %og_ref.1, f32[1,128]{1,0:T(1,128)} %reshape.9.stw_ref, ...), custom_call_target="tpu_custom_call" | custom-call | tf_op jit(solution)/shard_map/layer/pallas_call | solution.py:388
  104.9 1.5 %copy.16 = bf16[24,2048]{1,0:T(8,128)(2,1)} copy(bf16[24,2048]{1,0:T(8,128)(2,1)} %layer.1) | data formatting | bytes 196608
Async XLA Ops:
  0.0 0.7 copy-start

commit v2 on v1

--- a/solution.py
+++ b/solution.py
@@ -80,7 +80,7 @@
     left = jnp.concatenate([at, rt], 0)
     right = jnp.concatenate([ins * dn, k * dn], 0).astype(BF16)
     lane2 = iota((N, 256), 1) % 128
-    us, outs = [], []
+    us, reads = [], []
     for h in range(2):
         head_lanes = iota((2 * N, 128), 1) // 64 == h
         g = dot(jnp.where(head_lanes, left, 0.0), right, 1, 1)
@@ -90,20 +90,27 @@
         mrk = jnp.where(row >= col, g[N:, N:], 0.0)
         x = invert(low)
         u = dot(x, jnp.concatenate([at, dot(mak, v)], 1))
-        o = dot(mrb, u)
-        ov = dot(mrk, v)
         us.append(u)
-        outs.append(jnp.concatenate([o[:, :128] + rt, o[:, 128:] + ov], 1))
+        reads.append((mrb, mrk))
         service()
     u = jnp.where(lane2 < 64, us[0], us[1])
-    o = jnp.where(lane2 < 64, outs[0], outs[1])
     f = dot((ins * rest).T, u)
     fl = f[:, 128:] + dot((k * rest).T, v)
     ones = head_ones()
     r1, c1 = iota((128, 128), 0), iota((128, 128), 1)
     e = f[:, :128] * ones + jnp.where(r1 == c1, jnp.exp(last) - 1.0, 0.0)
     l = fl * ones
-    return e[:64] + e[64:], l[:64] + l[64:], o
+
+    def outputs():
+        outs = []
+        for h in range(2):
+            mrb, mrk = reads[h]
+            o = dot(mrb, us[h])
+            ov = dot(mrk, v)
+            outs.append(jnp.concatenate([o[:, :128] + rt, o[:, 128:] + ov], 1))
+        return jnp.where(lane2 < 64, outs[0], outs[1])
+
+    return e[:64] + e[64:], l[:64] + l[64:], outputs
 
 
 def unpack(p):
@@ -120,7 +127,7 @@
     r_ref, k_ref, v_ref, dec_ref, lr_ref, og_ref, stw_ref, hng_ref, wo_ref, res_ref, png_ref,
     wg_ref, wu_ref, wd_ref,
     out_ref,
-    gu, dn, state, entry_buf, part, pair_in, mine, mix_in, rows_buf, nrm, local_out, resid,
+    gu, dn, state, far, part, pair_in, mine, mix_in, relay, joint, rows_buf, nrm, local_out, resid,
     loc_sem, zs, zr, ys, yr, as_, ar, azs, azr, ss, sr, ps, pr, xs, xr, gs, gr, fs, fr,
 ):
     z, y, x, core = (lax.axis_index(a) for a in ("z", "y", "x", "c"))
@@ -236,29 +243,31 @@
     turn = [0]
 
     def service():
-        s = turn[0]
+        s, weighty = divmod(turn[0], 2)
         turn[0] += 1
-        if s == 0:
+        if s == 0 and not weighty:
             z_out(0)
-            for d in (1, 2, 3):
+            for d in (1, 3, 2):
                 push(dn.at[here], dn.at[here], as_.at[d - 1], ar.at[d - 1], at(dy=d))
             y_out(0)
-        elif s <= 8:
+        elif s <= 8 and not weighty:
             z_in(s)
             if s < 8:
                 z_out(s)
-            if s == 1:
+            for o in offsets(s):
+                y_out(o)
+        elif s <= 8:
+            if s == 0:
                 for d in (1, 2, 3):
                     landed(dn.at[slot(0, -d)], as_.at[d - 1], ar.at[d - 1])
             else:
-                a_in(s - 1)
-            a_out(s - 1)
-            for o in offsets(s):
-                y_out(o)
-            for o in offsets(s - 1):
-                y_on(o)
-        elif s == 9:
-            a_in(8)
+                a_in(s)
+            if s < 8:
+                a_out(s)
+            if s > 0:
+                for o in offsets(s - 1):
+                    y_on(o)
+        elif s == 9 and not weighty:
             for o in offsets(8):
                 y_on(o)
             for t in range(9):
@@ -267,16 +276,18 @@
 
     service()
 
-    e, l, o = local_scan(r_ref[...], k_ref[...], v_ref[...], dec_ref[...], lr_ref[...], service)
-    local_out[...] = o
-
-    def level(n, x_own, mates, place):
+    e, l, outputs = local_scan(
+        r_ref[...], k_ref[...], v_ref[...], dec_ref[...], lr_ref[...], service
+    )
+
+    def level(n, x_own, mates, place, meanwhile):
         state[n, place, :, :128] = x_own[0].astype(BF16)
         state[n, place, :, 128:] = x_own[1].astype(BF16)
-        for d in (1, 2, 3):
+        for d in (2, 1, 3):
             b = state.at[n, place]
             push(b, b, ss.at[n, d - 1], sr.at[n, d - 1], mates[d - 1])
-        for d in (1, 2, 3):
+        meanwhile()
+        for d in (1, 3, 2):
             landed(state.at[n, lax.rem(place - d + 4, 4)], ss.at[n, d - 1], sr.at[n, d - 1])
         total = unpack(state[n, 0].astype(F32))
         before = jnp.zeros_like(total)
@@ -286,15 +297,44 @@
             total = total + nxt + dot(nxt[:, :128], total)
         return total, before
 
+    def meanwhile_outputs():
+        local_out[...] = outputs()
+        service()
+
+    def meanwhile_services():
+        service()
+        service()
+
     y_mates = [at(dy=d) for d in (1, 2, 3)]
-    t1, b1 = level(0, (e, l), y_mates, y)
+    t1, b1 = level(0, (e, l), y_mates, y, meanwhile_outputs)
+    p1 = pack(t1)
+    t2, b2 = level(1, (p1[:, :128], p1[:, 128:]), z_near, zb, meanwhile_services)
+
+    p2 = pack(t2).astype(BF16)
+    quarter = jnp.zeros((16, 256), BF16)
+    for j in range(4):
+        quarter = jnp.where(y == j, p2[j * 16 : (j + 1) * 16], quarter)
+    far[za, y] = quarter
+    for d in (2, 1, 3):
+        b = far.at[za, y]
+        push(b, b, ss.at[2, d - 1], sr.at[2, d - 1], z_far[d - 1])
     service()
-    p1 = pack(t1)
-    t2, b2 = level(1, (p1[:, :128], p1[:, 128:]), z_near, zb)
     service()
-    p2 = pack(t2)
-    _, b3 = level(2, (p2[:, :128], p2[:, 128:]), z_far, za)
-    h0 = b3[:, 128:]
+    for d in (1, 3, 2):
+        landed(far.at[lax.rem(za - d + 4, 4), y], ss.at[2, d - 1], sr.at[2, d - 1])
+    for d in (2, 1, 3):
+        b = far.at[:, y]
+        push(b, b, ss.at[3, d - 1], sr.at[3, d - 1], y_mates[d - 1])
+    service()
+    for d in (1, 3, 2):
+        landed(far.at[:, lax.rem(y - d + 4, 4)], ss.at[3, d - 1], sr.at[3, d - 1])
+    total = unpack(far[0].reshape(64, 256)[:, 128:].astype(F32))
+    h0 = jnp.zeros_like(total)
+    for j in range(1, 4):
+        h0 = jnp.where(za == j, total, h0)
+        if j < 3:
+            nxt = unpack(far[j].reshape(64, 256).astype(F32))
+            total = total + nxt[:, 128:] + dot(nxt[:, :128], total)
     h0 = h0 + dot(b2[:, :128], h0) + b2[:, 128:]
     h0 = h0 + dot(b1[:, :128], h0) + b1[:, 128:]
 
@@ -318,20 +358,44 @@
                     p * ROWS : (p + 1) * ROWS
                 ].astype(BF16)
 
-    def scattered_sum(n):
+    halves = (pl.ds(0, D // 2), pl.ds(D // 2, D // 2))
+
+    def scattered_sum(n, meanwhile):
         other = 1 - core
-        for j in range(4):
-            push(part.at[j, other], pair_in.at[n, j], ps.at[n, j], pr.at[n, j], at(dc=1))
-        for d in (2, 1, 3, 0):
-            j = lax.rem(x + d, NX)
-            landed(pair_in.at[n, j], ps.at[n, j], pr.at[n, j])
+        across = lax.rem(x + 2, NX)
+        sides = (lax.rem(x + 1, NX), lax.rem(x + 3, NX))
+        steps = (at(dx=1), at(dx=-1))
+        order = (across, *sides, x)
+        for i, j in enumerate(order):
+            push(part.at[j, other], pair_in.at[n, j], ps.at[n, i], pr.at[n, i], at(dc=1))
+        for i, j in enumerate(order):
+            landed(pair_in.at[n, j], ps.at[n, i], pr.at[n, i])
             mine[n, j] = (part[j, core].astype(F32) + pair_in[n, j].astype(F32)).astype(BF16)
-            if d:
-                push(mine.at[n, j], mix_in.at[n, d - 1], xs.at[n, d - 1], xr.at[n, d - 1], at(dx=d))
+            if i == 0:
+                for e in range(2):
+                    push(mine.at[n, j, :, halves[e]], relay.at[n, e], xs.at[n, e], xr.at[n, e], steps[e])
+            elif i < 3:
+                cut = halves[2 - i]
+                push(
+                    mine.at[n, j, :, cut], mix_in.at[n, i - 1, :, cut], xs.at[n, 1 + i],
+                    xr.at[n, 1 + i], steps[i - 1],
+                )
+        meanwhile()
+        for e in range(2):
+            landed(relay.at[n, e], xs.at[n, e], xr.at[n, e])
+            joint[n, e] = (
+                mine[n, sides[e], :, halves[e]].astype(F32) + relay[n, e].astype(F32)
+            ).astype(BF16)
+            push(
+                joint.at[n, e], mix_in.at[n, e, :, halves[e]], xs.at[n, 4 + e], xr.at[n, 4 + e],
+                steps[e],
+            )
+        meanwhile()
         total = mine[n, x].astype(F32)
-        for d in (1, 3, 2):
-            landed(mix_in.at[n, d - 1], xs.at[n, d - 1], xr.at[n, d - 1])
-            total = total + mix_in[n, d - 1].astype(F32)
+        for e in range(2):
+            landed(mix_in.at[n, e, :, halves[1 - e]], xs.at[n, 2 + e], xr.at[n, 2 + e])
+            landed(mix_in.at[n, e, :, halves[e]], xs.at[n, 4 + e], xr.at[n, 4 + e])
+            total = total + mix_in[n, e].astype(F32)
         return total
 
     def finish_sends():
@@ -340,9 +404,7 @@
         sends.clear()
 
     shares(mixed, wo_ref[...], 0)
-    service()
-    mix = scattered_sum(0).astype(BF16).astype(F32)
-    service()
+    mix = scattered_sum(0, service).astype(BF16).astype(F32)
     fetch.wait()
     after = (resid[...].astype(F32) + mix).astype(BF16).astype(F32)
     factor = lax.rsqrt(jnp.mean(after * after, axis=-1, keepdims=True) + NORM_EPS)
@@ -350,21 +412,36 @@
 
     rows_buf[x, core] = normed
     mine_rows = rows_buf.at[x, core]
-    push(mine_rows, mine_rows, gs.at[0], gr.at[0], at(dc=1))
-    for d in (2, 1, 3):
-        push(mine_rows, mine_rows, gs.at[d], gr.at[d], at(dx=d))
-    for d in (1, 3, 2):
-        b = rows_buf.at[lax.rem(x + NX - d, NX), core]
-        landed(b, gs.at[d], gr.at[d])
-        push(b, b, fs.at[d - 1], fr.at[d - 1], at(dc=1))
+    for e in range(2):
+        b = rows_buf.at[x, core, :, halves[e]]
+        push(b, b, gs.at[e, 0], gr.at[e, 0], at(dx=1 if e == 0 else -1))
+    for e in range(2):
+        b = rows_buf.at[x, core, :, halves[1 - e]]
+        push(b, b, gs.at[e, 1], gr.at[e, 1], at(dx=1 if e == 0 else -1))
+    push(mine_rows, mine_rows, fs.at[0], fr.at[0], at(dc=1))
     service()
-    landed(rows_buf.at[x, 1 - core], gs.at[0], gr.at[0])
-    for d in (1, 3, 2):
-        b = rows_buf.at[lax.rem(x + NX - d, NX), 1 - core]
-        landed(b, fs.at[d - 1], fr.at[d - 1])
+
+    def came(dx, e, half, i, k, onward):
+        b = rows_buf.at[lax.rem(x + dx, NX), core, :, halves[half]]
+        landed(b, gs.at[e, i], gr.at[e, i])
+        if onward:
+            push(b, b, gs.at[e, 2], gr.at[e, 2], at(dx=1 if e == 0 else -1))
+        push(b, b, fs.at[k], fr.at[k], at(dc=1))
+
+    came(3, 0, 0, 0, 1, True)
+    came(1, 1, 1, 0, 2, True)
+    came(3, 0, 1, 1, 3, False)
+    came(1, 1, 0, 1, 4, False)
+    service()
+    came(2, 0, 0, 2, 5, False)
+    came(2, 1, 1, 2, 6, False)
+    landed(rows_buf.at[x, 1 - core], fs.at[0], fr.at[0])
+    for k, (dx, half) in enumerate(((3, 0), (1, 1), (3, 1), (1, 0), (2, 0), (2, 1))):
+        b = rows_buf.at[lax.rem(x + dx, NX), 1 - core, :, halves[half]]
+        landed(b, fs.at[k + 1], fr.at[k + 1])
     for j in range(8):
         nrm[j * ROWS : (j + 1) * ROWS] = rows_buf[j // 2, j % 2]
-    while turn[0] <= 9:
+    while turn[0] <= 18:
         service()
     finish_sends()
 
@@ -376,7 +453,7 @@
         upper = upper + dot(a, gu[j * 8 : (j + 1) * 8, W:].reshape(256, FF))
     hidden = (gate / (1.0 + jnp.exp(-gate)) * upper).astype(BF16)
     shares(hidden, dn[...].reshape(D, FF), 1)
-    down = scattered_sum(1)
+    down = scattered_sum(1, lambda: None)
     out_ref[...] = (after + down).astype(BF16)
     finish_sends()
 
@@ -393,12 +470,14 @@
         scratch_shapes=[
             pltpu.VMEM((64, 2 * W, FF), BF16),
             pltpu.VMEM((64, W, FF), BF16),
-            pltpu.VMEM((3, 4, 64, 256), BF16),
-            pltpu.VMEM((8, 128), F32),
+            pltpu.VMEM((2, 4, 64, 256), BF16),
+            pltpu.VMEM((4, NY, 16, 256), BF16),
             pltpu.VMEM((NX, NC, ROWS, D), BF16),
             pltpu.VMEM((2, NX, ROWS, D), BF16),
             pltpu.VMEM((2, NX, ROWS, D), BF16),
-            pltpu.VMEM((2, 3, ROWS, D), BF16),
+            pltpu.VMEM((2, 2, ROWS, D), BF16),
+            pltpu.VMEM((2, 2, ROWS, D // 2), BF16),
+            pltpu.VMEM((2, 2, ROWS, D // 2), BF16),
             pltpu.VMEM((NX, NC, ROWS, D), BF16),
             pltpu.VMEM((N, D), BF16),
             pltpu.VMEM((N, 256), F32),
@@ -408,11 +487,11 @@
             dma((16, 4)), dma((16, 4)),
             dma((3,)), dma((3,)),
             dma((2, 8)), dma((2, 8)),
-            dma((3, 3)), dma((3, 3)),
+            dma((4, 3)), dma((4, 3)),
             dma((2, 4)), dma((2, 4)),
+            dma((2, 6)), dma((2, 6)),
             dma((2, 3)), dma((2, 3)),
-            dma((4,)), dma((4,)),
-            dma((3,)), dma((3,)),
+            dma((7,)), dma((7,)),
         ],
         compiler_params=pltpu.CompilerParams(
             collective_id=0, has_side_effects=True, vmem_limit_bytes=60 * 1024 * 1024

time: 107 us -> 103 us (0.963)
  Pallas kernels: 104 us -> 100 us
    pallas_call x1, Pallas kernels: 104 us -> 100 us  [per_device(): pl.pallas_call(kernel, out_shape=jax.ShapeDtypeStruct((ROWS, D), BF16), i...]
where the time goes in v2:
time: 103 us
  Pallas kernels  100 us (97%)
  local copies, waits for them, and re-layouts  2.81 us (3%)
    pallas_call x1, Pallas kernels, per_device(): pl.pallas_call(kernel, out_shape=jax.ShapeDtypeStruct((ROWS, D), BF16), i...  100 us
    unnamed x3, local copies, waits for them, and re-layouts  2.22 us

profile of v2, /device:TPU:1, one launch (start us, length us, event | category | flops | bytes accessed | tf_op | source)
XLA Modules:
  0.0 103.0 jit_solution(2146377961386906396)
XLA Ops:
  0.0 0.0 copy-start
  0.0 0.7 copy-done
  0.7 0.6 reshape.9.stw_ref
  1.3 100.1 %layer.1 = bf16[24,2048]{1,0:T(8,128)(2,1)} custom-call(bf16[192,128]{1,0:T(8,128)(2,1)} %r_ref.1, bf16[192,128]{1,0:T(8,128)(2,1)} %k_ref.1, bf16[192,128]{1,0:T(8,128)(2,1)} %v_ref.1, f32[192,128]{1,0:T(8,128)} %dec_ref.1, f32[192,128]{1,0:T(8,128)} %lr_ref.1, bf16[192,128]{1,0:T(8,128)(2,1)} %og_ref.1, f32[1,128]{1,0:T(1,128)} %reshape.9.stw_ref, ...), custom_call_target="tpu_custom_call" | custom-call | tf_op jit(solution)/shard_map/layer/pallas_call | solution.py:465
  101.4 1.5 %copy.16 = bf16[24,2048]{1,0:T(8,128)(2,1)} copy(bf16[24,2048]{1,0:T(8,128)(2,1)} %layer.1) | data formatting | bytes 196608
Async XLA Ops:
  0.0 0.7 copy-start

commit v3 on v2

--- a/solution.py
+++ b/solution.py
@@ -21,6 +21,8 @@
 D = 2048
 FF = 640
 W = 32
+TURNS = 28
+POINTS = 19
 
 
 def dot(a, b, ca=1, cb=0):
@@ -89,10 +91,12 @@
         mrb = jnp.where(row >= col, g[N:, :N], 0.0)
         mrk = jnp.where(row >= col, g[N:, N:], 0.0)
         x = invert(low)
+        service()
         u = dot(x, jnp.concatenate([at, dot(mak, v)], 1))
         us.append(u)
         reads.append((mrb, mrk))
-        service()
+        if h == 1:
+            service()
     u = jnp.where(lane2 < 64, us[0], us[1])
     f = dot((ins * rest).T, u)
     fl = f[:, 128:] + dot((k * rest).T, v)
@@ -227,47 +231,54 @@
         for d in range(2):
             landed(z_block(-s if d == 0 else s, d, s), zs.at[d, s - 1], zr.at[d, s - 1])
 
-    def a_block(dz, d, s):
-        return dn.at[pl.ds(column(dz), NY)] if s < 8 else dn.at[pl.ds(column(dz) + 2 * d, 2)]
-
-    def a_out(s):
-        for d in range(2):
-            b = a_block(-s if d == 0 else s, d, s + 1)
-            push(b, b, azs.at[d, s], azr.at[d, s], at(dz=1 if d == 0 else -1))
-
-    def a_in(s):
-        for d in range(2):
-            b = a_block(-s if d == 0 else s, d, s)
-            landed(b, azs.at[d, s - 1], azr.at[d, s - 1])
-
-    turn = [0]
+    def a_dirs(s, g):
+        return (0, 1) if s < 8 else (g,)
+
+    def a_block(s, d, g):
+        return dn.at[pl.ds(column(-s if d == 0 else s) + 2 * g, 2)]
+
+    def a_out(s, g):
+        for d in a_dirs(s + 1, g):
+            b = a_block(s, d, g)
+            push(b, b, azs.at[d, g, s], azr.at[d, g, s], at(dz=1 if d == 0 else -1))
+
+    def a_in(s, g):
+        for d in a_dirs(s, g):
+            landed(a_block(s, d, g), azs.at[d, g, s - 1], azr.at[d, g, s - 1])
+
+    turn, points = [0], [0]
 
     def service():
-        s, weighty = divmod(turn[0], 2)
+        points[0] += 1
+        while turn[0] < min(points[0] * TURNS // POINTS, TURNS):
+            one_turn()
+
+    def one_turn():
+        s, g = divmod(turn[0], 3)
         turn[0] += 1
-        if s == 0 and not weighty:
+        if s == 0 and g == 0:
             z_out(0)
             for d in (1, 3, 2):
                 push(dn.at[here], dn.at[here], as_.at[d - 1], ar.at[d - 1], at(dy=d))
             y_out(0)
-        elif s <= 8 and not weighty:
+        elif s <= 8 and g == 0:
             z_in(s)
             if s < 8:
                 z_out(s)
             for o in offsets(s):
                 y_out(o)
         elif s <= 8:
-            if s == 0:
+            if s == 0 and g == 1:
                 for d in (1, 2, 3):
                     landed(dn.at[slot(0, -d)], as_.at[d - 1], ar.at[d - 1])
-            else:
-                a_in(s)
+            if s > 0:
+                a_in(s, g - 1)
             if s < 8:
-                a_out(s)
+                a_out(s, g - 1)
             if s > 0:
-                for o in offsets(s - 1):
+                for o in offsets(s - 1)[g - 1 : g]:
                     y_on(o)
-        elif s == 9 and not weighty:
+        else:
             for o in offsets(8):
                 y_on(o)
             for t in range(9):
@@ -298,6 +309,7 @@
         return total, before
 
     def meanwhile_outputs():
+        service()
         local_out[...] = outputs()
         service()
 
@@ -368,6 +380,7 @@
         order = (across, *sides, x)
         for i, j in enumerate(order):
             push(part.at[j, other], pair_in.at[n, j], ps.at[n, i], pr.at[n, i], at(dc=1))
+        meanwhile()
         for i, j in enumerate(order):
             landed(pair_in.at[n, j], ps.at[n, i], pr.at[n, i])
             mine[n, j] = (part[j, core].astype(F32) + pair_in[n, j].astype(F32)).astype(BF16)
@@ -403,6 +416,7 @@
             cp.wait_send()
         sends.clear()
 
+    service()
     shares(mixed, wo_ref[...], 0)
     mix = scattered_sum(0, service).astype(BF16).astype(F32)
     fetch.wait()
@@ -420,6 +434,7 @@
         push(b, b, gs.at[e, 1], gr.at[e, 1], at(dx=1 if e == 0 else -1))
     push(mine_rows, mine_rows, fs.at[0], fr.at[0], at(dc=1))
     service()
+    service()
 
     def came(dx, e, half, i, k, onward):
         b = rows_buf.at[lax.rem(x + dx, NX), core, :, halves[half]]
@@ -441,8 +456,8 @@
         landed(b, fs.at[k + 1], fr.at[k + 1])
     for j in range(8):
         nrm[j * ROWS : (j + 1) * ROWS] = rows_buf[j // 2, j % 2]
-    while turn[0] <= 18:
-        service()
+    while turn[0] < TURNS:
+        one_turn()
     finish_sends()
 
     gate = jnp.zeros((N, FF), F32)
@@ -486,7 +501,7 @@
             dma((2, 8)), dma((2, 8)),
             dma((16, 4)), dma((16, 4)),
             dma((3,)), dma((3,)),
-            dma((2, 8)), dma((2, 8)),
+            dma((2, 2, 8)), dma((2, 2, 8)),
             dma((4, 3)), dma((4, 3)),
             dma((2, 4)), dma((2, 4)),
             dma((2, 6)), dma((2, 6)),

time: 103 us -> 96.1 us (0.933)
  Pallas kernels: 100 us -> 92.6 us
    pallas_call x1, Pallas kernels: 100 us -> 92.6 us  [per_device(): pl.pallas_call(kernel, out_shape=jax.ShapeDtypeStruct((ROWS, D), BF16), i...]
where the time goes in v3:
time: 96.1 us; the launch traced here: 95.5 us
  Pallas kernels  92.6 us (96%)
  local copies, waits for them, and re-layouts  2.81 us (3%)
    pallas_call x1, Pallas kernels, per_device(): pl.pallas_call(kernel, out_shape=jax.ShapeDtypeStruct((ROWS, D), BF16), i...  92.6 us
    unnamed x3, local copies, waits for them, and re-layouts  2.22 us

profile of v3, /device:TPU:1, one launch (start us, length us, event | category | flops | bytes accessed | tf_op | source)
XLA Modules:
  0.0 95.5 jit_solution(4674352087293247645)
XLA Ops:
  0.0 0.0 copy-start
  0.0 0.7 copy-done
  0.7 0.6 reshape.9.stw_ref
  1.3 92.6 %layer.1 = bf16[24,2048]{1,0:T(8,128)(2,1)} custom-call(bf16[192,128]{1,0:T(8,128)(2,1)} %r_ref.1, bf16[192,128]{1,0:T(8,128)(2,1)} %k_ref.1, bf16[192,128]{1,0:T(8,128)(2,1)} %v_ref.1, f32[192,128]{1,0:T(8,128)} %dec_ref.1, f32[192,128]{1,0:T(8,128)} %lr_ref.1, bf16[192,128]{1,0:T(8,128)(2,1)} %og_ref.1, f32[1,128]{1,0:T(1,128)} %reshape.9.stw_ref, ...), custom_call_target="tpu_custom_call" | custom-call | tf_op jit(solution)/shard_map/layer/pallas_call | solution.py:480
  93.9 1.5 %copy.16 = bf16[24,2048]{1,0:T(8,128)(2,1)} copy(bf16[24,2048]{1,0:T(8,128)(2,1)} %layer.1) | data formatting | bytes 196608
Async XLA Ops:
  0.0 0.7 copy-start

commit v4 on v3

--- a/solution.py
+++ b/solution.py
@@ -132,7 +132,7 @@
     wg_ref, wu_ref, wd_ref,
     out_ref,
     gu, dn, state, far, part, pair_in, mine, mix_in, relay, joint, rows_buf, nrm, local_out, resid,
-    loc_sem, zs, zr, ys, yr, as_, ar, azs, azr, ss, sr, ps, pr, xs, xr, gs, gr, fs, fr,
+    loc_sem, word, zs, zr, ys, yr, as_, ar, azs, azr, ss, sr, ps, pr, xs, xr, gs, gr, fs, fr,
 ):
     z, y, x, core = (lax.axis_index(a) for a in ("z", "y", "x", "c"))
     here = z * NY + y
@@ -173,16 +173,26 @@
 
     zb, za = z % 4, z // 4
     peers = [at(dz=1), at(dz=-1), at(dy=1), at(dy=2), at(dy=3)]
-    peers += [at(dx=d) for d in (1, 2, 3)] + [at(dc=1)]
+    peers += [at(dx=1), at(dx=-1), at(dc=1)]
     z_near = [(za * 4 + lax.rem(zb + d, 4), y, x, core) for d in (1, 2, 3)]
     z_far = [at(dz=4 * d) for d in (1, 2, 3)]
-    peers += z_near + z_far
     barrier = pltpu.get_barrier_semaphore()
     for p in peers:
         pl.semaphore_signal(barrier, inc=1, device_id=p, device_id_type=MESH)
     for cp in own:
         cp.wait()
     pl.semaphore_wait(barrier, len(peers))
+
+    def word_on(t):
+        for d in range(2):
+            to = at(dz=1 if d == 0 else -1)
+            pl.semaphore_signal(word.at[d, t], inc=1, device_id=to, device_id_type=MESH)
+
+    def word_in(t):
+        for d in range(2):
+            pl.semaphore_wait(word.at[d, t], 1)
+
+    word_on(0)
 
     def slot(dz, dy=0):
         return lax.rem(z + dz + NZ, NZ) * NY + lax.rem(y + dy + NY, NY)
@@ -256,6 +266,10 @@
     def one_turn():
         s, g = divmod(turn[0], 3)
         turn[0] += 1
+        if 2 <= turn[0] <= 8:
+            word_in(turn[0] - 2)
+            if turn[0] < 8:
+                word_on(turn[0] - 1)
         if s == 0 and g == 0:
             z_out(0)
             for d in (1, 3, 2):
@@ -497,7 +511,7 @@
             pltpu.VMEM((N, D), BF16),
             pltpu.VMEM((N, 256), F32),
             pltpu.VMEM((ROWS, D), BF16),
-            dma((4,)),
+            dma((4,)), pltpu.SemaphoreType.REGULAR((2, 7)),
             dma((2, 8)), dma((2, 8)),
             dma((16, 4)), dma((16, 4)),
             dma((3,)), dma((3,)),

time: 96.1 us -> 93.6 us (0.974)
  Pallas kernels: 92.6 us -> 90.1 us
    pallas_call x1, Pallas kernels: 92.6 us -> 90.1 us  [per_device(): pl.pallas_call(kernel, out_shape=jax.ShapeDtypeStruct((ROWS, D), BF16), i...]
where the time goes in v4:
time: 93.6 us; the launch traced here: 92.9 us
  Pallas kernels  90.1 us (96%)
  local copies, waits for them, and re-layouts  2.81 us (3%)
    pallas_call x1, Pallas kernels, per_device(): pl.pallas_call(kernel, out_shape=jax.ShapeDtypeStruct((ROWS, D), BF16), i...  90.1 us
    unnamed x3, local copies, waits for them, and re-layouts  2.22 us

profile of v4, /device:TPU:1, one launch (start us, length us, event | category | flops | bytes accessed | tf_op | source)
XLA Modules:
  0.0 92.9 jit_solution(8454540164969274545)
XLA Ops:
  0.0 0.0 copy-start
  0.0 0.7 copy-done
  0.7 0.6 reshape.9.stw_ref
  1.3 90.1 %layer.1 = bf16[24,2048]{1,0:T(8,128)(2,1)} custom-call(bf16[192,128]{1,0:T(8,128)(2,1)} %r_ref.1, bf16[192,128]{1,0:T(8,128)(2,1)} %k_ref.1, bf16[192,128]{1,0:T(8,128)(2,1)} %v_ref.1, f32[192,128]{1,0:T(8,128)} %dec_ref.1, f32[192,128]{1,0:T(8,128)} %lr_ref.1, bf16[192,128]{1,0:T(8,128)(2,1)} %og_ref.1, f32[1,128]{1,0:T(1,128)} %reshape.9.stw_ref, ...), custom_call_target="tpu_custom_call" | custom-call | tf_op jit(solution)/shard_map/layer/pallas_call | solution.py:494
  91.3 1.5 %copy.16 = bf16[24,2048]{1,0:T(8,128)(2,1)} copy(bf16[24,2048]{1,0:T(8,128)(2,1)} %layer.1) | data formatting | bytes 196608
Async XLA Ops:
  0.0 0.7 copy-start

commit v5 on v4

--- a/solution.py
+++ b/solution.py
@@ -128,11 +128,12 @@
 
 
 def kernel(
-    r_ref, k_ref, v_ref, dec_ref, lr_ref, og_ref, stw_ref, hng_ref, wo_ref, res_ref, png_ref,
+    r_in, k_in, v_in, dec_in, lr_in, og_in, stw_in, hng_in, wo_in, res_ref, png_in,
     wg_ref, wu_ref, wd_ref,
     out_ref,
+    r_ref, k_ref, v_ref, dec_ref, lr_ref, og_ref, stw_ref, hng_ref, wo_ref, png_ref,
     gu, dn, state, far, part, pair_in, mine, mix_in, relay, joint, rows_buf, nrm, local_out, resid,
-    loc_sem, word, zs, zr, ys, yr, as_, ar, azs, azr, ss, sr, ps, pr, xs, xr, gs, gr, fs, fr,
+    loc_sem, in_sem, word, zs, zr, ys, yr, as_, ar, azs, azr, ss, sr, ps, pr, xs, xr, gs, gr, fs, fr,
 ):
     z, y, x, core = (lax.axis_index(a) for a in ("z", "y", "x", "c"))
     here = z * NY + y
@@ -167,9 +168,6 @@
     ]
     row0 = pl.multiple_of((x * NC + core) * ROWS, 8)
     fetch = pltpu.make_async_copy(res_ref.at[pl.ds(row0, ROWS)], resid, loc_sem.at[3])
-    for cp in own:
-        cp.start()
-    fetch.start()
 
     zb, za = z % 4, z // 4
     peers = [at(dz=1), at(dz=-1), at(dy=1), at(dy=2), at(dy=3)]
@@ -179,6 +177,13 @@
     barrier = pltpu.get_barrier_semaphore()
     for p in peers:
         pl.semaphore_signal(barrier, inc=1, device_id=p, device_id_type=MESH)
+    pairs = (
+        (r_in, r_ref), (k_in, k_ref), (v_in, v_ref), (dec_in, dec_ref), (lr_in, lr_ref),
+        (og_in, og_ref), (stw_in, stw_ref), (hng_in, hng_ref), (wo_in, wo_ref), (png_in, png_ref),
+    )
+    staged = [pltpu.make_async_copy(a, b, in_sem.at[i]) for i, (a, b) in enumerate(pairs)]
+    for cp in (*own, *staged, fetch):
+        cp.start()
     for cp in own:
         cp.wait()
     pl.semaphore_wait(barrier, len(peers))
@@ -295,11 +300,11 @@
         else:
             for o in offsets(8):
                 y_on(o)
-            for t in range(9):
-                for o in offsets(t):
-                    y_end(o)
-
-    service()
+
+    service()
+
+    for cp in staged[:5]:
+        cp.wait()
 
     e, l, outputs = local_scan(
         r_ref[...], k_ref[...], v_ref[...], dec_ref[...], lr_ref[...], service
@@ -364,49 +369,65 @@
     h0 = h0 + dot(b2[:, :128], h0) + b2[:, 128:]
     h0 = h0 + dot(b1[:, :128], h0) + b1[:, 128:]
 
+    for cp in staged[5:]:
+        cp.wait()
+    own_weight = jnp.concatenate([stw_ref[0:1], stw_ref[1:2]], 1)
     o = local_out[...]
     mech = dot(o[:, :128], h0) + o[:, 128:]
     ones = head_ones()
     rf, kf, vf = r_ref[...].astype(F32), k_ref[...].astype(F32), v_ref[...].astype(F32)
     centred = mech - dotx(mech, ones) * (1.0 / 64)
     spread = dotx(centred * centred, ones) * (1.0 / 64)
-    token = dotx(rf * kf * stw_ref[...], ones) * vf
+    token = dotx(rf * kf * own_weight, ones) * vf
     mixed = centred * lax.rsqrt(spread + GROUP_EPS) * hng_ref[...] + token
     mixed = (mixed / (1.0 + jnp.exp(-og_ref[...].astype(F32)))).astype(BF16)
 
-    def shares(a, b, cb):
-        for j in range(4):
-            cols = D // 4 * j
-            bj = b[:, cols : cols + D // 4] if cb == 0 else b[cols : cols + D // 4]
-            prod = dot(a, bj, 1, cb)
-            for p in range(8):
-                part[p // 2, p % 2, :, cols : cols + D // 4] = prod[
-                    p * ROWS : (p + 1) * ROWS
-                ].astype(BF16)
-
     halves = (pl.ds(0, D // 2), pl.ds(D // 2, D // 2))
-
-    def scattered_sum(n, meanwhile):
+    Q = D // 4
+
+    def sum_over_tp(n, a, columns_of, cb, meanwhile):
         other = 1 - core
         across = lax.rem(x + 2, NX)
         sides = (lax.rem(x + 1, NX), lax.rem(x + 3, NX))
         steps = (at(dx=1), at(dx=-1))
-        order = (across, *sides, x)
-        for i, j in enumerate(order):
-            push(part.at[j, other], pair_in.at[n, j], ps.at[n, i], pr.at[n, i], at(dc=1))
+
+        def product(q):
+            cut = pl.ds(q * Q, Q)
+            prod = dot(a, columns_of(q * Q), 1, cb)
+            for p in range(8):
+                part[p // 2, p % 2, :, cut] = prod[p * ROWS : (p + 1) * ROWS].astype(BF16)
+            push(
+                part.at[:, other, :, cut], pair_in.at[n, :, :, cut], ps.at[n, q], pr.at[n, q],
+                at(dc=1),
+            )
+
+        def add_pair(q):
+            cut = pl.ds(q * Q, Q)
+            landed(pair_in.at[n, :, :, cut], ps.at[n, q], pr.at[n, q])
+            mine[n, :, :, cut] = (
+                part[:, core, :, cut].astype(F32) + pair_in[n, :, :, cut].astype(F32)
+            ).astype(BF16)
+
+        def first_sends(e):
+            push(
+                mine.at[n, across, :, halves[e]], relay.at[n, e], xs.at[n, e], xr.at[n, e], steps[e]
+            )
+            push(
+                mine.at[n, sides[1 - e], :, halves[e]], mix_in.at[n, 1 - e, :, halves[e]],
+                xs.at[n, 3 - e], xr.at[n, 3 - e], steps[1 - e],
+            )
+
+        product(0)
+        product(1)
+        add_pair(0)
+        product(2)
+        add_pair(1)
+        first_sends(0)
+        product(3)
         meanwhile()
-        for i, j in enumerate(order):
-            landed(pair_in.at[n, j], ps.at[n, i], pr.at[n, i])
-            mine[n, j] = (part[j, core].astype(F32) + pair_in[n, j].astype(F32)).astype(BF16)
-            if i == 0:
-                for e in range(2):
-                    push(mine.at[n, j, :, halves[e]], relay.at[n, e], xs.at[n, e], xr.at[n, e], steps[e])
-            elif i < 3:
-                cut = halves[2 - i]
-                push(
-                    mine.at[n, j, :, cut], mix_in.at[n, i - 1, :, cut], xs.at[n, 1 + i],
-                    xr.at[n, 1 + i], steps[i - 1],
-                )
+        add_pair(2)
+        add_pair(3)
+        first_sends(1)
         meanwhile()
         for e in range(2):
             landed(relay.at[n, e], xs.at[n, e], xr.at[n, e])
@@ -431,8 +452,8 @@
         sends.clear()
 
     service()
-    shares(mixed, wo_ref[...], 0)
-    mix = scattered_sum(0, service).astype(BF16).astype(F32)
+    mix = sum_over_tp(0, mixed, lambda c: wo_ref[:, c : c + Q], 0, service)
+    mix = mix.astype(BF16).astype(F32)
     fetch.wait()
     after = (resid[...].astype(F32) + mix).astype(BF16).astype(F32)
     factor = lax.rsqrt(jnp.mean(after * after, axis=-1, keepdims=True) + NORM_EPS)
@@ -470,19 +491,28 @@
         landed(b, fs.at[k + 1], fr.at[k + 1])
     for j in range(8):
         nrm[j * ROWS : (j + 1) * ROWS] = rows_buf[j // 2, j % 2]
-    while turn[0] < TURNS:
-        one_turn()
-    finish_sends()
 
     gate = jnp.zeros((N, FF), F32)
     upper = jnp.zeros((N, FF), F32)
+    arrivals = [o for t in range(9) for o in offsets(t)]
     for j in range(8):
-        a = nrm[:, j * 256 : (j + 1) * 256]
-        gate = gate + dot(a, gu[j * 8 : (j + 1) * 8, :W].reshape(256, FF))
-        upper = upper + dot(a, gu[j * 8 : (j + 1) * 8, W:].reshape(256, FF))
+        s_last = abs(arrivals[2 * j + 1])
+        while turn[0] < min(3 * (s_last + 1) + 3, TURNS):
+            one_turn()
+        if turn[0] < TURNS:
+            one_turn()
+        two = arrivals[2 * j : 2 * j + 2]
+        for o in two:
+            y_end(o)
+        cuts = [pl.ds(pl.multiple_of(lax.rem(z + o + NZ, NZ) * 128, 128), 128) for o in two]
+        a = jnp.concatenate([nrm[:, cut] for cut in cuts], 1)
+        wide = [gu[pl.ds(column(o), NY)] for o in two]
+        gate = gate + dot(a, jnp.concatenate([w[:, :W].reshape(128, FF) for w in wide], 0))
+        upper = upper + dot(a, jnp.concatenate([w[:, W:].reshape(128, FF) for w in wide], 0))
+    assert turn[0] == TURNS
     hidden = (gate / (1.0 + jnp.exp(-gate)) * upper).astype(BF16)
-    shares(hidden, dn[...].reshape(D, FF), 1)
-    down = scattered_sum(1, lambda: None)
+    finish_sends()
+    down = sum_over_tp(1, hidden, lambda c: dn[c // W : (c + Q) // W].reshape(Q, FF), 1, lambda: None)
     out_ref[...] = (after + down).astype(BF16)
     finish_sends()
 
@@ -494,9 +524,16 @@
     return pl.pallas_call(
         kernel,
         out_shape=jax.ShapeDtypeStruct((ROWS, D), BF16),
-        in_specs=[vmem] * 9 + [hbm] + [vmem] + [hbm] * 3,
+        in_specs=[hbm] * 14,
         out_specs=vmem,
         scratch_shapes=[
+            *[pltpu.VMEM((N, 128), BF16)] * 3,
+            *[pltpu.VMEM((N, 128), F32)] * 2,
+            pltpu.VMEM((N, 128), BF16),
+            pltpu.VMEM((2, 64), F32),
+            pltpu.VMEM((1, 128), F32),
+            pltpu.VMEM((128, D), BF16),
+            pltpu.VMEM((1, D), F32),
             pltpu.VMEM((64, 2 * W, FF), BF16),
             pltpu.VMEM((64, W, FF), BF16),
             pltpu.VMEM((2, 4, 64, 256), BF16),
@@ -511,7 +548,7 @@
             pltpu.VMEM((N, D), BF16),
             pltpu.VMEM((N, 256), F32),
             pltpu.VMEM((ROWS, D), BF16),
-            dma((4,)), pltpu.SemaphoreType.REGULAR((2, 7)),
+            dma((4,)), dma((10,)), pltpu.SemaphoreType.REGULAR((2, 7)),
             dma((2, 8)), dma((2, 8)),
             dma((16, 4)), dma((16, 4)),
             dma((3,)), dma((3,)),
@@ -526,7 +563,7 @@
             collective_id=0, has_side_effects=True, vmem_limit_bytes=60 * 1024 * 1024
         ),
         name="layer",
-    )(r, k, v, dec, lr, og, stw.reshape(1, 128), hng.reshape(1, 128), wo, res,
+    )(r, k, v, dec, lr, og, stw, hng.reshape(1, 128), wo, res,
       png.reshape(1, D), wg, wu, wd.T)
 
 

time: 93.6 us -> 90.1 us (0.963)
  Pallas kernels: 90.1 us -> 88.3 us
  local copies, waits for them, and re-layouts: 2.81 us -> 1.54 us
    pallas_call x1, Pallas kernels: 90.1 us -> 88.3 us  [per_device(): pl.pallas_call(kernel, out_shape=jax.ShapeDtypeStruct((ROWS, D), BF16), i...]
    unnamed x3 -> x1, local copies, waits for them, and re-layouts: 2.22 us -> 1.54 us
where the time goes in v5:
time: 90.1 us; the launch traced here: 89.8 us
  Pallas kernels  88.3 us (98%)
  local copies, waits for them, and re-layouts  1.54 us (2%)
    pallas_call x1, Pallas kernels, per_device(): pl.pallas_call(kernel, out_shape=jax.ShapeDtypeStruct((ROWS, D), BF16), i...  88.3 us

profile of v5, /device:TPU:1, one launch (start us, length us, event | category | flops | bytes accessed | tf_op | source)
XLA Modules:
  0.0 89.8 jit_solution(6059629456405541414)
XLA Ops:
  0.0 88.3 %layer.1 = bf16[24,2048]{1,0:T(8,128)(2,1)} custom-call(bf16[192,128]{1,0:T(8,128)(2,1)} %r_in.1, bf16[192,128]{1,0:T(8,128)(2,1)} %k_in.1, bf16[192,128]{1,0:T(8,128)(2,1)} %v_in.1, f32[192,128]{1,0:T(8,128)} %dec_in.1, f32[192,128]{1,0:T(8,128)} %lr_in.1, bf16[192,128]{1,0:T(8,128)(2,1)} %og_in.1, f32[2,64]{1,0:T(2,128)} %stw_in.1, f32[1,128]{1,0:T(1,128)} %bitcast.5, ...), custom_call_target="tpu_custom_call" | custom-call | tf_op jit(solution)/shard_map/layer/pallas_call | solution.py:524
  88.3 1.5 %copy.16 = bf16[24,2048]{1,0:T(8,128)(2,1)} copy(bf16[24,2048]{1,0:T(8,128)(2,1)} %layer.1) | data formatting | bytes 196608

commit v6 on v5

--- a/solution.py
+++ b/solution.py
@@ -10,7 +10,6 @@
 from jax.sharding import PartitionSpec as P
 
 F32, BF16 = jnp.float32, jnp.bfloat16
-EXACT = lax.Precision.HIGHEST
 MESH = pl.DeviceIdType.MESH
 GROUP_EPS = 0.00064
 NORM_EPS = 1e-06
@@ -22,7 +21,7 @@
 FF = 640
 W = 32
 TURNS = 28
-POINTS = 19
+PLAN = (1, 2, 4, 4, 7, 8, 10, 11, 13, 14, 16, 17, 19, 20, 22, 23, 25, 26)
 
 
 def dot(a, b, ca=1, cb=0):
@@ -31,10 +30,28 @@
     )
 
 
-def dotx(a, b, ca=1, cb=0):
-    return lax.dot_general(
-        a, b, (((ca,), (cb,)), ((), ())), precision=EXACT, preferred_element_type=F32
-    )
+def split(a):
+    high = a.astype(BF16)
+    return high, (a - high.astype(F32)).astype(BF16)
+
+
+def dot3(a, b):
+    (ah, al), (bh, bl) = split(a), split(b)
+    return dot(ah, bh) + (dot(ah, bl) + dot(al, bh))
+
+
+def head_sums(a):
+    high, low = split(a)
+    ones = head_ones().astype(BF16)
+    return dot(jnp.concatenate([high, low], 1), jnp.concatenate([ones, ones], 0))
+
+
+def running_sums(a):
+    n = a.shape[0]
+    high, low = split(a)
+    tri = jnp.where(iota((n, n), 0) >= iota((n, n), 1), 1.0, 0.0).astype(BF16)
+    sums = dot(tri, jnp.concatenate([high, low], 1))
+    return sums[:, : a.shape[1]] + sums[:, a.shape[1] :]
 
 
 def iota(shape, d):
@@ -50,11 +67,11 @@
     row, col = iota((n, n), 0), iota((n, n), 1)
     eye = jnp.where(row == col, 1.0, 0.0).astype(F32)
     d = jnp.where(row // 8 == col // 8, low, 0.0)
-    d2 = dotx(d, d)
-    d4 = dotx(d2, d2)
+    d2 = dot3(d, d)
+    d4 = dot3(d2, d2)
     x = eye + d
-    x = x + dotx(d2, x)
-    x = x + dotx(d4, x)
+    x = x + dot3(d2, x)
+    x = x + dot3(d4, x)
     m = 8
     while m < 64:
         off = jnp.where((row // (2 * m) == col // (2 * m)) & (row // m != col // m), low, 0.0)
@@ -70,8 +87,8 @@
     r, k, v = r.astype(F32), k.astype(F32), v.astype(F32)
     lw = (-math.exp(-0.5)) / (1.0 + jnp.exp(-dec))
     row, col = iota((N, N), 0), iota((N, N), 1)
-    c = dotx(jnp.where(row >= col, 1.0, 0.0).astype(F32), lw)
-    norm = jnp.sqrt(dotx(k * k, head_ones()))
+    c = running_sums(lw)
+    norm = jnp.sqrt(head_sums(k * k))
     unit = k / jnp.maximum(norm, 1.0)
     ins = unit / (1.0 + jnp.exp(-lr))
     up, dn = jnp.exp(c), jnp.exp(-c)
@@ -117,6 +134,10 @@
     return e[:64] + e[64:], l[:64] + l[64:], outputs
 
 
+def after_of(first, then):
+    return first + then + dot(then[:, :128], first)
+
+
 def unpack(p):
     first = iota(p.shape, 1) % 128 < 64
     return jnp.concatenate([jnp.where(first, p, 0.0), jnp.where(first, 0.0, p)], 0)
@@ -132,7 +153,7 @@
     wg_ref, wu_ref, wd_ref,
     out_ref,
     r_ref, k_ref, v_ref, dec_ref, lr_ref, og_ref, stw_ref, hng_ref, wo_ref, png_ref,
-    gu, dn, state, far, part, pair_in, mine, mix_in, relay, joint, rows_buf, nrm, local_out, resid,
+    gu, dn, state, far, part, pair_in, mine, mix_in, rows_buf, nrm, local_out, resid,
     loc_sem, in_sem, word, zs, zr, ys, yr, as_, ar, azs, azr, ss, sr, ps, pr, xs, xr, gs, gr, fs, fr,
 ):
     z, y, x, core = (lax.axis_index(a) for a in ("z", "y", "x", "c"))
@@ -144,7 +165,7 @@
             lax.rem(x + dx + NX, NX), lax.rem(core + dc, NC),
         )
 
-    sends = []
+    sends, pair_sends = [], []
 
     def push(src, dst, send, recv, to):
         cp = pltpu.make_async_remote_copy(
@@ -171,7 +192,7 @@
 
     zb, za = z % 4, z // 4
     peers = [at(dz=1), at(dz=-1), at(dy=1), at(dy=2), at(dy=3)]
-    peers += [at(dx=1), at(dx=-1), at(dc=1)]
+    peers += [at(dx=1), at(dx=2), at(dx=3), at(dc=1)]
     z_near = [(za * 4 + lax.rem(zb + d, 4), y, x, core) for d in (1, 2, 3)]
     z_far = [at(dz=4 * d) for d in (1, 2, 3)]
     barrier = pltpu.get_barrier_semaphore()
@@ -190,7 +211,7 @@
 
     def word_on(t):
         for d in range(2):
-            to = at(dz=1 if d == 0 else -1)
+            to = at(dz=2**t if d == 0 else -(2**t))
             pl.semaphore_signal(word.at[d, t], inc=1, device_id=to, device_id_type=MESH)
 
     def word_in(t):
@@ -265,16 +286,17 @@
 
     def service():
         points[0] += 1
-        while turn[0] < min(points[0] * TURNS // POINTS, TURNS):
+        while turn[0] < PLAN[points[0] - 1]:
             one_turn()
 
     def one_turn():
         s, g = divmod(turn[0], 3)
         turn[0] += 1
-        if 2 <= turn[0] <= 8:
-            word_in(turn[0] - 2)
-            if turn[0] < 8:
-                word_on(turn[0] - 1)
+        if turn[0] in (2, 4):
+            word_in(turn[0] // 2 - 1)
+            word_on(turn[0] // 2)
+        if turn[0] == 7:
+            word_in(2)
         if s == 0 and g == 0:
             z_out(0)
             for d in (1, 3, 2):
@@ -319,12 +341,11 @@
         meanwhile()
         for d in (1, 3, 2):
             landed(state.at[n, lax.rem(place - d + 4, 4)], ss.at[n, d - 1], sr.at[n, d - 1])
-        total = unpack(state[n, 0].astype(F32))
-        before = jnp.zeros_like(total)
-        for j in range(1, 4):
-            before = jnp.where(place == j, total, before)
-            nxt = unpack(state[n, j].astype(F32))
-            total = total + nxt + dot(nxt[:, :128], total)
+        m = [unpack(state[n, j].astype(F32)) for j in range(4)]
+        m01, m23 = after_of(m[0], m[1]), after_of(m[2], m[3])
+        m012, total = after_of(m01, m[2]), after_of(m01, m23)
+        before = jnp.where(place == 1, m[0], jnp.zeros_like(total))
+        before = jnp.where(place == 2, m01, jnp.where(place == 3, m012, before))
         return total, before
 
     def meanwhile_outputs():
@@ -374,11 +395,10 @@
     own_weight = jnp.concatenate([stw_ref[0:1], stw_ref[1:2]], 1)
     o = local_out[...]
     mech = dot(o[:, :128], h0) + o[:, 128:]
-    ones = head_ones()
     rf, kf, vf = r_ref[...].astype(F32), k_ref[...].astype(F32), v_ref[...].astype(F32)
-    centred = mech - dotx(mech, ones) * (1.0 / 64)
-    spread = dotx(centred * centred, ones) * (1.0 / 64)
-    token = dotx(rf * kf * own_weight, ones) * vf
+    centred = mech - head_sums(mech) * (1.0 / 64)
+    spread = head_sums(centred * centred) * (1.0 / 64)
+    token = head_sums(rf * kf * own_weight) * vf
     mixed = centred * lax.rsqrt(spread + GROUP_EPS) * hng_ref[...] + token
     mixed = (mixed / (1.0 + jnp.exp(-og_ref[...].astype(F32)))).astype(BF16)
 
@@ -387,19 +407,18 @@
 
     def sum_over_tp(n, a, columns_of, cb, meanwhile):
         other = 1 - core
-        across = lax.rem(x + 2, NX)
-        sides = (lax.rem(x + 1, NX), lax.rem(x + 3, NX))
-        steps = (at(dx=1), at(dx=-1))
 
         def product(q):
             cut = pl.ds(q * Q, Q)
             prod = dot(a, columns_of(q * Q), 1, cb)
             for p in range(8):
                 part[p // 2, p % 2, :, cut] = prod[p * ROWS : (p + 1) * ROWS].astype(BF16)
-            push(
+            cp = push(
                 part.at[:, other, :, cut], pair_in.at[n, :, :, cut], ps.at[n, q], pr.at[n, q],
                 at(dc=1),
             )
+            if n == 0:
+                pair_sends.append(cp)
 
         def add_pair(q):
             cut = pl.ds(q * Q, Q)
@@ -409,13 +428,11 @@
             ).astype(BF16)
 
         def first_sends(e):
-            push(
-                mine.at[n, across, :, halves[e]], relay.at[n, e], xs.at[n, e], xr.at[n, e], steps[e]
-            )
-            push(
-                mine.at[n, sides[1 - e], :, halves[e]], mix_in.at[n, 1 - e, :, halves[e]],
-                xs.at[n, 3 - e], xr.at[n, 3 - e], steps[1 - e],
-            )
+            for d in (2, 1, 3):
+                push(
+                    mine.at[n, lax.rem(x + d, NX), :, halves[e]], mix_in.at[n, d - 1, :, halves[e]],
+                    xs.at[n, e, d - 1], xr.at[n, e, d - 1], at(dx=d),
+                )
 
         product(0)
         product(1)
@@ -429,21 +446,12 @@
         add_pair(3)
         first_sends(1)
         meanwhile()
-        for e in range(2):
-            landed(relay.at[n, e], xs.at[n, e], xr.at[n, e])
-            joint[n, e] = (
-                mine[n, sides[e], :, halves[e]].astype(F32) + relay[n, e].astype(F32)
-            ).astype(BF16)
-            push(
-                joint.at[n, e], mix_in.at[n, e, :, halves[e]], xs.at[n, 4 + e], xr.at[n, 4 + e],
-                steps[e],
-            )
         meanwhile()
         total = mine[n, x].astype(F32)
-        for e in range(2):
-            landed(mix_in.at[n, e, :, halves[1 - e]], xs.at[n, 2 + e], xr.at[n, 2 + e])
-            landed(mix_in.at[n, e, :, halves[e]], xs.at[n, 4 + e], xr.at[n, 4 + e])
-            total = total + mix_in[n, e].astype(F32)
+        for d in (1, 3, 2):
+            for e in range(2):
+                landed(mix_in.at[n, d - 1, :, halves[e]], xs.at[n, e, d - 1], xr.at[n, e, d - 1])
+            total = total + mix_in[n, d - 1].astype(F32)
         return total
 
     def finish_sends():
@@ -461,34 +469,18 @@
 
     rows_buf[x, core] = normed
     mine_rows = rows_buf.at[x, core]
-    for e in range(2):
-        b = rows_buf.at[x, core, :, halves[e]]
-        push(b, b, gs.at[e, 0], gr.at[e, 0], at(dx=1 if e == 0 else -1))
-    for e in range(2):
-        b = rows_buf.at[x, core, :, halves[1 - e]]
-        push(b, b, gs.at[e, 1], gr.at[e, 1], at(dx=1 if e == 0 else -1))
+    for d in (2, 1, 3):
+        push(mine_rows, mine_rows, gs.at[d - 1], gr.at[d - 1], at(dx=d))
     push(mine_rows, mine_rows, fs.at[0], fr.at[0], at(dc=1))
     service()
     service()
-
-    def came(dx, e, half, i, k, onward):
-        b = rows_buf.at[lax.rem(x + dx, NX), core, :, halves[half]]
-        landed(b, gs.at[e, i], gr.at[e, i])
-        if onward:
-            push(b, b, gs.at[e, 2], gr.at[e, 2], at(dx=1 if e == 0 else -1))
-        push(b, b, fs.at[k], fr.at[k], at(dc=1))
-
-    came(3, 0, 0, 0, 1, True)
-    came(1, 1, 1, 0, 2, True)
-    came(3, 0, 1, 1, 3, False)
-    came(1, 1, 0, 1, 4, False)
-    service()
-    came(2, 0, 0, 2, 5, False)
-    came(2, 1, 1, 2, 6, False)
-    landed(rows_buf.at[x, 1 - core], fs.at[0], fr.at[0])
-    for k, (dx, half) in enumerate(((3, 0), (1, 1), (3, 1), (1, 0), (2, 0), (2, 1))):
-        b = rows_buf.at[lax.rem(x + dx, NX), 1 - core, :, halves[half]]
-        landed(b, fs.at[k + 1], fr.at[k + 1])
+    for d in (1, 3, 2):
+        b = rows_buf.at[lax.rem(x + NX - d, NX), core]
+        landed(b, gs.at[d - 1], gr.at[d - 1])
+        push(b, b, fs.at[d], fr.at[d], at(dc=1))
+    service()
+    for d in (0, 1, 3, 2):
+        landed(rows_buf.at[lax.rem(x + NX - d, NX), 1 - core], fs.at[d], fr.at[d])
     for j in range(8):
         nrm[j * ROWS : (j + 1) * ROWS] = rows_buf[j // 2, j % 2]
 
@@ -511,7 +503,9 @@
         upper = upper + dot(a, jnp.concatenate([w[:, W:].reshape(128, FF) for w in wide], 0))
     assert turn[0] == TURNS
     hidden = (gate / (1.0 + jnp.exp(-gate)) * upper).astype(BF16)
-    finish_sends()
+    for cp in pair_sends:
+        cp.wait_send()
+    sends[:] = [cp for cp in sends if all(cp is not p for p in pair_sends)]
     down = sum_over_tp(1, hidden, lambda c: dn[c // W : (c + Q) // W].reshape(Q, FF), 1, lambda: None)
     out_ref[...] = (after + down).astype(BF16)
     finish_sends()
@@ -541,23 +535,21 @@
             pltpu.VMEM((NX, NC, ROWS, D), BF16),
             pltpu.VMEM((2, NX, ROWS, D), BF16),
             pltpu.VMEM((2, NX, ROWS, D), BF16),
-            pltpu.VMEM((2, 2, ROWS, D), BF16),
-            pltpu.VMEM((2, 2, ROWS, D // 2), BF16),
-            pltpu.VMEM((2, 2, ROWS, D // 2), BF16),
+            pltpu.VMEM((2, 3, ROWS, D), BF16),
             pltpu.VMEM((NX, NC, ROWS, D), BF16),
             pltpu.VMEM((N, D), BF16),
             pltpu.VMEM((N, 256), F32),
             pltpu.VMEM((ROWS, D), BF16),
-            dma((4,)), dma((10,)), pltpu.SemaphoreType.REGULAR((2, 7)),
+            dma((4,)), dma((10,)), pltpu.SemaphoreType.REGULAR((2, 3)),
             dma((2, 8)), dma((2, 8)),
             dma((16, 4)), dma((16, 4)),
             dma((3,)), dma((3,)),
             dma((2, 2, 8)), dma((2, 2, 8)),
             dma((4, 3)), dma((4, 3)),
             dma((2, 4)), dma((2, 4)),
-            dma((2, 6)), dma((2, 6)),
-            dma((2, 3)), dma((2, 3)),
-            dma((7,)), dma((7,)),
+            dma((2, 2, 3)), dma((2, 2, 3)),
+            dma((3,)), dma((3,)),
+            dma((4,)), dma((4,)),
         ],
         compiler_params=pltpu.CompilerParams(
             collective_id=0, has_side_effects=True, vmem_limit_bytes=60 * 1024 * 1024

time: 90.1 us -> 88.2 us (0.979)
  Pallas kernels: 88.3 us -> 86.5 us
    pallas_call x1, Pallas kernels: 88.3 us -> 86.5 us  [per_device(): pl.pallas_call(kernel, out_shape=jax.ShapeDtypeStruct((ROWS, D), BF16), i...]
where the time goes in v6:
time: 88.2 us; the launch traced here: 88.1 us
  Pallas kernels  86.5 us (98%)
  local copies, waits for them, and re-layouts  1.54 us (2%)
    pallas_call x1, Pallas kernels, per_device(): pl.pallas_call(kernel, out_shape=jax.ShapeDtypeStruct((ROWS, D), BF16), i...  86.5 us

profile of v6, /device:TPU:1, one launch (start us, length us, event | category | flops | bytes accessed | tf_op | source)
XLA Modules:
  0.0 88.1 jit_solution(10374432095333842709)
XLA Ops:
  0.0 86.5 %layer.1 = bf16[24,2048]{1,0:T(8,128)(2,1)} custom-call(bf16[192,128]{1,0:T(8,128)(2,1)} %r_in.1, bf16[192,128]{1,0:T(8,128)(2,1)} %k_in.1, bf16[192,128]{1,0:T(8,128)(2,1)} %v_in.1, f32[192,128]{1,0:T(8,128)} %dec_in.1, f32[192,128]{1,0:T(8,128)} %lr_in.1, bf16[192,128]{1,0:T(8,128)(2,1)} %og_in.1, f32[2,64]{1,0:T(2,128)} %stw_in.1, f32[1,128]{1,0:T(1,128)} %bitcast.5, ...), custom_call_target="tpu_custom_call" | custom-call | tf_op jit(solution)/shard_map/layer/pallas_call | solution.py:518
  86.5 1.5 %copy.16 = bf16[24,2048]{1,0:T(8,128)(2,1)} copy(bf16[24,2048]{1,0:T(8,128)(2,1)} %layer.1) | data formatting | bytes 196608

commit v7 on v6

--- a/solution.py
+++ b/solution.py
@@ -309,6 +309,9 @@
             for o in offsets(s):
                 y_out(o)
         elif s <= 8:
+            if s > 0:
+                for o in offsets(s - 1)[g - 1 : g]:
+                    y_on(o)
             if s == 0 and g == 1:
                 for d in (1, 2, 3):
                     landed(dn.at[slot(0, -d)], as_.at[d - 1], ar.at[d - 1])
@@ -316,9 +319,6 @@
                 a_in(s, g - 1)
             if s < 8:
                 a_out(s, g - 1)
-            if s > 0:
-                for o in offsets(s - 1)[g - 1 : g]:
-                    y_on(o)
         else:
             for o in offsets(8):
                 y_on(o)

time: 88.2 us -> 88.3 us (level)
  no operation moved by 1% of the time
where the time goes in v7:
time: 88.3 us; the launch traced here: 88.1 us
  Pallas kernels  86.6 us (98%)
  local copies, waits for them, and re-layouts  1.54 us (2%)
    pallas_call x1, Pallas kernels, per_device(): pl.pallas_call(kernel, out_shape=jax.ShapeDtypeStruct((ROWS, D), BF16), i...  86.6 us

profile of v7, /device:TPU:1, one launch (start us, length us, event | category | flops | bytes accessed | tf_op | source)
XLA Modules:
  0.0 88.1 jit_solution(2550464744358848732)
XLA Ops:
  0.0 86.6 %layer.1 = bf16[24,2048]{1,0:T(8,128)(2,1)} custom-call(bf16[192,128]{1,0:T(8,128)(2,1)} %r_in.1, bf16[192,128]{1,0:T(8,128)(2,1)} %k_in.1, bf16[192,128]{1,0:T(8,128)(2,1)} %v_in.1, f32[192,128]{1,0:T(8,128)} %dec_in.1, f32[192,128]{1,0:T(8,128)} %lr_in.1, bf16[192,128]{1,0:T(8,128)(2,1)} %og_in.1, f32[2,64]{1,0:T(2,128)} %stw_in.1, f32[1,128]{1,0:T(1,128)} %bitcast.5, ...), custom_call_target="tpu_custom_call" | custom-call | tf_op jit(solution)/shard_map/layer/pallas_call | solution.py:518
  86.6 1.5 %copy.16 = bf16[24,2048]{1,0:T(8,128)(2,1)} copy(bf16[24,2048]{1,0:T(8,128)(2,1)} %layer.1) | data formatting | bytes 196608
